TPU v7x, 256 devices: a whole 4x4x8 slice. The times are simulated.
256 devices in a mesh: sp: 32 (over z, x), tp: 8 (over y, core).
Axes of the slice: x: 4, y: 4, z: 8, core: 2. Of those that a mesh axis runs over, the one named last changes fastest.
Arguments:
- tokens: bfloat16 [16384, 2048], P(('sp', 'tp')), may hold values from -6 to 6
- norm_gain: float32 [2048], replicated, may hold values from 0.1 to 1.9
- w_query: bfloat16 [2048, 1024], P(None, 'tp'), may hold values from -16 to 16
- w_key: bfloat16 [2048, 1024], P(None, 'tp'), may hold values from -16 to 16
- w_value: bfloat16 [2048, 1024], P(None, 'tp'), may hold values from -0.125 to 0.125
- conv_in: bfloat16 [2048, 2048], P(None, 'tp'), may hold values from -0.125 to 0.125
- conv_gate: bfloat16 [2048, 2048], P(None, 'tp'), may hold values from -0.125 to 0.125
- conv_taps: float32 [31, 2048], P(None, 'tp'), may hold values from -3.7 to 3.7
- conv_gain: float32 [2048], P('tp'), may hold values from 0.1 to 1.9
- cum_gate: float32 [16, 16384], P('tp'), may hold values from -2050 to 0, as said below
- out_attn: bfloat16 [1024, 2048], P('tp'), may hold values from -0.75 to 0.75
- out_conv: bfloat16 [2048, 2048], P('tp'), may hold values from -0.125 to 0.125
Outputs:
- mixed: bfloat16 [16384, 2048], P(('sp', 'tp'))
- log_total: float32 [16, 16384], P('tp', 'sp')
Inputs may be any that keep to these rules, and one draw needn't show every extreme that they name: `cum_gate`: for each head the values never rise from one position to the next and are at most 0.
All inputs are finite; a program needn't handle non-finite values.
Results may differ from a plain program's by a relative error of at most 0.014.
Values may be sent and summed in bfloat16 or wider, within the bound.
A program may use at most 128 MiB of HBM per device.

v0:
```python
import jax
import jax.numpy as jnp
from jax import lax
from jax.sharding import PartitionSpec as P

HEAD = 64


def from_everyone(array, axis):
    length = lax.axis_size(axis)
    return lax.all_to_all(
        jnp.broadcast_to(array[None], (length, *array.shape)), axis, 0, 0, tiled=True
    )


def laid_out(pieces, dim):
    dims = list(pieces.shape[1:])
    dims[dim] *= pieces.shape[0]
    return jnp.moveaxis(pieces, 0, dim).reshape(dims)


def gather_directly(array, axis, dim):
    pieces = from_everyone(array, axis)
    return laid_out(pieces, dim)


def sent_together(arrays, axis, dim, along):
    both = jnp.concatenate(arrays, axis=along)
    result, at, done = (lax.all_gather(both, axis, axis=dim, tiled=True), 0, [])
    for a in arrays:
        done.append(lax.slice_in_dim(result, at, at + a.shape[along], axis=along))
        at += a.shape[along]
    return tuple(done)


def shifted(array, axis, by):
    length = lax.axis_size(axis)
    pairs = [(i, i + by) for i in range(length) if 0 <= i + by < length]
    return lax.ppermute(array, axis, pairs)


def over_copies(array, axis):
    everything = from_everyone(array, axis)
    return jnp.sum(everything, axis=0)


def split_up(array, dim, length):
    before, after = (array.shape[:dim], array.shape[dim + 1 :])
    return jnp.moveaxis(array.reshape(*before, length, -1, *after), dim, 0)


def sent_and_summed(array, axis, dim):
    length = lax.axis_size(axis)
    pieces = lax.all_to_all(split_up(array, dim, length), axis, 0, 0, tiled=True)
    return jnp.sum(pieces.astype(jnp.float32), axis=0)


def per_device(
    tokens,
    norm_gain,
    w_query,
    w_key,
    w_value,
    conv_in,
    conv_gate,
    conv_taps,
    conv_gain,
    cum_gate,
    out_attn,
    out_conv,
):
    heads_here = w_query.shape[1] // HEAD
    width_att = w_query.shape[1]
    channels = conv_in.shape[1]
    kernel_len = conv_taps.shape[0]
    wide = gather_directly(tokens, "tp", 0).astype(jnp.float32)
    factor = lax.rsqrt(jnp.mean(wide * wide, axis=1, keepdims=True) + 1e-06)
    normed = (wide * factor * norm_gain[None, :]).astype(jnp.bfloat16)
    query = (jnp.dot(normed, w_query, preferred_element_type=jnp.float32) * HEAD ** (-0.5)).astype(
        jnp.bfloat16
    )
    keyed = jnp.dot(normed, w_key, preferred_element_type=jnp.float32).astype(jnp.bfloat16)
    valued = jnp.dot(normed, w_value, preferred_element_type=jnp.float32).astype(jnp.bfloat16)
    opened = jnp.dot(normed, conv_in, preferred_element_type=jnp.float32)
    gating = jnp.dot(normed, conv_gate, preferred_element_type=jnp.float32)
    gated_rows = (opened * jax.nn.sigmoid(gating)).astype(jnp.bfloat16)
    joined = jnp.concatenate([query, keyed, valued, gated_rows], axis=1)
    local_rows = joined.shape[0]
    own_index = lax.axis_index("sp")
    offset = own_index * local_rows
    query_rows = joined[:, :width_att]
    key_rows = joined[:, width_att : 2 * width_att]
    value_rows = joined[:, 2 * width_att : 3 * width_att]
    gated = joined[:, 3 * width_att :]
    group_list = (query_rows, offset)
    group_data = []
    group_rows, group_start = group_list
    count_rows = group_rows.shape[0]
    group_data.append(
        (
            group_rows.reshape(count_rows, heads_here, HEAD),
            lax.dynamic_slice_in_dim(cum_gate, group_start, count_rows, 1),
            group_start + jnp.arange(count_rows, dtype=jnp.int32),
            group_start + count_rows - 1,
        )
    )

    def absorb(carry_in, group, key_block, value_block, first_place):
        query_heads, cum_query, query_place, last_query = group
        row_best, row_total, row_accum = carry_in
        length_in = key_block.shape[0]
        key_heads = key_block.reshape(length_in, heads_here, HEAD)
        value_heads = value_block.reshape(length_in, heads_here, HEAD)
        cum_keys = lax.dynamic_slice_in_dim(cum_gate, first_place, length_in, 1)
        scores = jnp.einsum(
            "qhd,khd->hqk", query_heads, key_heads, preferred_element_type=jnp.float32
        )
        scores = scores + cum_query[:, :, None] - cum_keys[:, None, :]
        key_place = first_place + jnp.arange(length_in, dtype=jnp.int32)
        visible = jnp.logical_and(
            key_place[None, :] <= query_place[:, None], key_place[None, :] >= 0
        )[None]
        scores = jnp.where(visible, scores, -1e30)
        new_best = jnp.maximum(row_best, jnp.max(scores, axis=2))
        shrink = jnp.exp(row_best - new_best)
        weights = jnp.where(visible, jnp.exp(scores - new_best[:, :, None]), 0.0)
        row_total = shrink * row_total + jnp.sum(weights, axis=2)
        row_accum = shrink[:, :, None] * row_accum + jnp.einsum(
            "hqk,khd->hqd",
            weights.astype(jnp.bfloat16),
            value_heads,
            preferred_element_type=jnp.float32,
        )
        return (new_best, row_total, row_accum)

    initial = tuple(
        (
            (
                jnp.full((heads_here, group[0].shape[0]), -1e30, jnp.float32),
                jnp.zeros((heads_here, group[0].shape[0]), jnp.float32),
                jnp.zeros((heads_here, group[0].shape[0], HEAD), jnp.float32),
            )
            for group in group_data
        )
    )
    pieces = sent_together((key_rows, value_rows), "sp", 0, 1)
    key_group = pieces[0]
    value_group = pieces[1]
    length_in = key_group.shape[0]
    turns = length_in // local_rows

    def advance(turn_index, carry_now):
        begin_row = turn_index * local_rows
        key_block = lax.dynamic_slice_in_dim(key_group, begin_row, local_rows, 0)
        value_block = lax.dynamic_slice_in_dim(value_group, begin_row, local_rows, 0)
        updated = []
        for group, inner_carry in zip(group_data, carry_now):
            wanted = jnp.logical_and(begin_row <= group[3], begin_row + local_rows > 0)

            def take_block(inner, group=group):
                return absorb(inner, group, key_block, value_block, begin_row)

            def skip_block(inner):
                return inner

            updated.append(lax.cond(wanted, take_block, skip_block, inner_carry))
        return tuple(updated)

    carry = lax.fori_loop(0, turns, advance, initial)
    attended_parts = []
    total_parts = []
    for row_best, row_total, row_accum in carry:
        count_rows = row_total.shape[1]
        attended_parts.append(
            (row_accum / row_total[:, :, None])
            .astype(jnp.bfloat16)
            .transpose(1, 0, 2)
            .reshape(count_rows, width_att)
        )
        total_parts.append(row_best + jnp.log(row_total))
    attended = attended_parts[0]
    log_total = total_parts[0]
    rim_rows = shifted(gated[local_rows - (kernel_len - 1) :], "sp", 1)
    padded = jnp.concatenate([rim_rows, gated], axis=0).astype(jnp.float32)
    convolved = jnp.zeros((local_rows, channels), jnp.float32)
    for tap_index in range(kernel_len):
        convolved = (
            convolved + conv_taps[tap_index][None, :] * padded[tap_index : tap_index + local_rows]
        )
    all_channels = channels * lax.axis_size("tp")
    channel_square = over_copies(jnp.sum(convolved * convolved, axis=1), "tp") / all_channels
    conv_out = jax.nn.silu(
        convolved * lax.rsqrt(channel_square + 1e-06)[:, None] * conv_gain[None, :]
    ).astype(jnp.bfloat16)
    group_part = jnp.dot(attended, out_attn, preferred_element_type=jnp.float32)
    group_part = group_part + jnp.dot(conv_out, out_conv, preferred_element_type=jnp.float32)
    mixed = sent_and_summed(
        lax.optimization_barrier(group_part.astype(jnp.bfloat16))
        .astype(jnp.float32)
        .astype(jnp.bfloat16),
        "tp",
        0,
    ).astype(jnp.bfloat16)
    return (mixed, log_total)


def solution(mesh):
    in_specs = (
        P(("sp", "tp"), None),
        P(),
        P(None, "tp"),
        P(None, "tp"),
        P(None, "tp"),
        P(None, "tp"),
        P(None, "tp"),
        P(None, "tp"),
        P("tp"),
        P("tp", None),
        P("tp", None),
        P("tp", None),
    )
    out_specs = (P(("sp", "tp"), None), P("tp", "sp"))
    return jax.shard_map(
        per_device, mesh=mesh, in_specs=in_specs, out_specs=out_specs, check_vma=False
    )
```

profile of v0, /device:TPU:230, one launch (start us, length us, event | category | flops | bytes accessed | tf_op | source)
XLA Modules:
  0.0 319.2 jit_solution(631611161656552048)
XLA Ops:
  8.5 31.5 %all_to_all.16 = bf16[8,64,2048]{2,1,0:T(8,128)(2,1)S(1)} all-to-all(bf16[8,64,2048]{2,1,0:T(8,128)(2,1)S(1)} %broadcast_in_dim.65), channel_id=1, replica_groups=mesh['sp'=32,'tp'=8] {'tp'}, dimensions={0} | all-to-all | bytes 4194304 | tf_op jit(solution)/shard_map/all_to_all | solution.py:11
  40.0 1.3 copy-done.1
  42.0 2.2 fusion.10
  47.5 2.0 fusion.13
  52.9 3.0 collective-permute-done
  56.0 3.6 %multiply_reduce_fusion.1 = (f32[512]{0:T(512)S(1)}, f32[512,256]{1,0:T(8,128)}) fusion(f32[542,256]{1,0:T(8,128)S(1)} %maximum_convert_fusion, f32[256]{0:T(256)S(1)} %bitcast.77, f32[256]{0:T(256)S(1)} %bitcast.78, f32[256]{0:T(256)S(1)} %bitcast.80, f32[256]{0:T(256)S(1)} %bitcast.81, f32[256]{0:T(256)S(1)} %bitcast.82, f32[256]{0:T(256)S(1)} %bitcast.83, ...), kind=kLoop, calls=%fused_computation.96 | loop fusion | flops 8257024 | bytes 16811008 | tf_op jit(solution)/shard_map/reduce_sum | solution.py:191
  60.2 3.3 %all-to-all-start.1 = ((f32[8,1,512]{2,1,0:T(1,128)}), f32[8,1,512]{2,1,0:T(1,128)S(1)}, u32[]{:S(2)}, u32[]{:S(2)}) async-start(f32[8,1,512]{2,1,0:T(1,128)} %broadcast_in_dim.66), calls=%async_computation.1 | async-start | bytes 32768 | tf_op jit(solution)/shard_map/all_to_all | solution.py:11
  63.5 1.9 fusion.15
  65.4 3.4 %all-to-all-done.1 = f32[8,1,512]{2,1,0:T(1,128)S(1)} async-done(((f32[8,1,512]{2,1,0:T(1,128)}), f32[8,1,512]{2,1,0:T(1,128)S(1)}, u32[]{:S(2)}, u32[]{:S(2)}) %all-to-all-start.1) | async-done | bytes 16416 | tf_op jit(solution)/shard_map/all_to_all | solution.py:11
  68.8 3.8 %fusion.46 = f32[512,2048]{1,0:T(8,128)} fusion(bf16[256,2048]{1,0:T(8,128)(2,1)S(1)} %copy-done, f32[512,256]{1,0:T(8,128)} %get-tuple-element.380, f32[256]{0:T(256)S(1)} %copy-done.8, f32[512]{0:T(512)S(1)} %add_rsqrt_fusion.1), kind=kOutput, calls=%fused_computation.98 | convolution fusion | flops 537788416 | bytes 5770240 | tf_op jit(solution)/shard_map/dot_general | solution.py:196
  72.7 73.0 %all-gather.2.cloned.1.call-done = bf16[16384,256]{0,1:T(8,128)(2,1)} async-done(((bf16[512,256]{0,1:T(8,128)(2,1)}), bf16[16384,256]{0,1:T(8,128)(2,1)}) %all-gather.2.cloned.1.call-update) | async-done | bytes 8388624 | tf_op jit(solution)/shard_map/all_gather | solution.py:29
  145.6 5.8 %fusion.53 = (bf16[16384,128]{0,1:T(8,128)(2,1)}, bf16[16384,128]{0,1:T(8,128)(2,1)}) fusion(bf16[16384,256]{0,1:T(8,128)(2,1)} %all-gather.2.cloned.1.call-done), kind=kLoop, calls=%fused_computation.110 | loop fusion | bytes 16777216 | tf_op jit(solution)/shard_map/slice | solution.py:31
  151.5 124.0 %while.18 = (s32[]{:T(128)}, f32[2,512]{1,0:T(2,128)S(1)}, f32[2,512]{1,0:T(2,128)S(1)}, f32[2,512,64]{1,2,0:T(8,128)S(1)}, s32[]{:T(128)}, /*index=5*/bf16[1638...) while((s32[]{:T(128)}, f32[2,512]{1,0:T(2,128)S(1)}, ...), condition=%wide.region_6.7_spmd.clone, body=%wide.region_1.6_spmd.clone.sunk | while | flops 140120064 | bytes 8877437 | solution.py:169
  151.6 3.9 %conditional.3 = ((f32[2,512]{1,0:T(2,128)S(1)}, f32[2,512]{1,0:T(2,128)S(1)}, f32[2,512,64]{1,2,0:T(8,128)S(1)})) conditional(s32[]{:T(128)} %convert_element_type.82, (f32[2,512]{1,0:T(2,128)S(1)}, f32[2,512]{1,0:T(2,128)S(1)}, f32[2,512,64]{1,2,0:T(8,128)S(1)}) %tuple.88, (s32[]{:T(128)}, s32[]{:T(128)}, bf16[16384,128]{0,1:T(8,128)(2,1)}, ...), branch_computations={%region_2.0_spmd, %region_3.5_spmd} | conditional | flops 140120064 | bytes 8875094 | solution.py:166
  155.5 3.8 %conditional.3 = ((f32[2,512]{1,0:T(2,128)S(1)}, f32[2,512]{1,0:T(2,128)S(1)}, f32[2,512,64]{1,2,0:T(8,128)S(1)})) conditional(s32[]{:T(128)} %convert_element_type.82, (f32[2,512]{1,0:T(2,128)S(1)}, f32[2,512]{1,0:T(2,128)S(1)}, f32[2,512,64]{1,2,0:T(8,128)S(1)}) %tuple.88, (s32[]{:T(128)}, s32[]{:T(128)}, bf16[16384,128]{0,1:T(8,128)(2,1)}, ...), branch_computations={%region_2.0_spmd, %region_3.5_spmd} | conditional | flops 140120064 | bytes 8875094 | solution.py:166
  159.4 3.8 %conditional.3 = ((f32[2,512]{1,0:T(2,128)S(1)}, f32[2,512]{1,0:T(2,128)S(1)}, f32[2,512,64]{1,2,0:T(8,128)S(1)})) conditional(s32[]{:T(128)} %convert_element_type.82, (f32[2,512]{1,0:T(2,128)S(1)}, f32[2,512]{1,0:T(2,128)S(1)}, f32[2,512,64]{1,2,0:T(8,128)S(1)}) %tuple.88, (s32[]{:T(128)}, s32[]{:T(128)}, bf16[16384,128]{0,1:T(8,128)(2,1)}, ...), branch_computations={%region_2.0_spmd, %region_3.5_spmd} | conditional | flops 140120064 | bytes 8875094 | solution.py:166
  163.2 3.8 %conditional.3 = ((f32[2,512]{1,0:T(2,128)S(1)}, f32[2,512]{1,0:T(2,128)S(1)}, f32[2,512,64]{1,2,0:T(8,128)S(1)})) conditional(s32[]{:T(128)} %convert_element_type.82, (f32[2,512]{1,0:T(2,128)S(1)}, f32[2,512]{1,0:T(2,128)S(1)}, f32[2,512,64]{1,2,0:T(8,128)S(1)}) %tuple.88, (s32[]{:T(128)}, s32[]{:T(128)}, bf16[16384,128]{0,1:T(8,128)(2,1)}, ...), branch_computations={%region_2.0_spmd, %region_3.5_spmd} | conditional | flops 140120064 | bytes 8875094 | solution.py:166
  167.1 3.8 %conditional.3 = ((f32[2,512]{1,0:T(2,128)S(1)}, f32[2,512]{1,0:T(2,128)S(1)}, f32[2,512,64]{1,2,0:T(8,128)S(1)})) conditional(s32[]{:T(128)} %convert_element_type.82, (f32[2,512]{1,0:T(2,128)S(1)}, f32[2,512]{1,0:T(2,128)S(1)}, f32[2,512,64]{1,2,0:T(8,128)S(1)}) %tuple.88, (s32[]{:T(128)}, s32[]{:T(128)}, bf16[16384,128]{0,1:T(8,128)(2,1)}, ...), branch_computations={%region_2.0_spmd, %region_3.5_spmd} | conditional | flops 140120064 | bytes 8875094 | solution.py:166
  171.0 3.8 %conditional.3 = ((f32[2,512]{1,0:T(2,128)S(1)}, f32[2,512]{1,0:T(2,128)S(1)}, f32[2,512,64]{1,2,0:T(8,128)S(1)})) conditional(s32[]{:T(128)} %convert_element_type.82, (f32[2,512]{1,0:T(2,128)S(1)}, f32[2,512]{1,0:T(2,128)S(1)}, f32[2,512,64]{1,2,0:T(8,128)S(1)}) %tuple.88, (s32[]{:T(128)}, s32[]{:T(128)}, bf16[16384,128]{0,1:T(8,128)(2,1)}, ...), branch_computations={%region_2.0_spmd, %region_3.5_spmd} | conditional | flops 140120064 | bytes 8875094 | solution.py:166
  174.9 3.8 %conditional.3 = ((f32[2,512]{1,0:T(2,128)S(1)}, f32[2,512]{1,0:T(2,128)S(1)}, f32[2,512,64]{1,2,0:T(8,128)S(1)})) conditional(s32[]{:T(128)} %convert_element_type.82, (f32[2,512]{1,0:T(2,128)S(1)}, f32[2,512]{1,0:T(2,128)S(1)}, f32[2,512,64]{1,2,0:T(8,128)S(1)}) %tuple.88, (s32[]{:T(128)}, s32[]{:T(128)}, bf16[16384,128]{0,1:T(8,128)(2,1)}, ...), branch_computations={%region_2.0_spmd, %region_3.5_spmd} | conditional | flops 140120064 | bytes 8875094 | solution.py:166
  178.7 3.8 %conditional.3 = ((f32[2,512]{1,0:T(2,128)S(1)}, f32[2,512]{1,0:T(2,128)S(1)}, f32[2,512,64]{1,2,0:T(8,128)S(1)})) conditional(s32[]{:T(128)} %convert_element_type.82, (f32[2,512]{1,0:T(2,128)S(1)}, f32[2,512]{1,0:T(2,128)S(1)}, f32[2,512,64]{1,2,0:T(8,128)S(1)}) %tuple.88, (s32[]{:T(128)}, s32[]{:T(128)}, bf16[16384,128]{0,1:T(8,128)(2,1)}, ...), branch_computations={%region_2.0_spmd, %region_3.5_spmd} | conditional | flops 140120064 | bytes 8875094 | solution.py:166
  182.6 3.8 %conditional.3 = ((f32[2,512]{1,0:T(2,128)S(1)}, f32[2,512]{1,0:T(2,128)S(1)}, f32[2,512,64]{1,2,0:T(8,128)S(1)})) conditional(s32[]{:T(128)} %convert_element_type.82, (f32[2,512]{1,0:T(2,128)S(1)}, f32[2,512]{1,0:T(2,128)S(1)}, f32[2,512,64]{1,2,0:T(8,128)S(1)}) %tuple.88, (s32[]{:T(128)}, s32[]{:T(128)}, bf16[16384,128]{0,1:T(8,128)(2,1)}, ...), branch_computations={%region_2.0_spmd, %region_3.5_spmd} | conditional | flops 140120064 | bytes 8875094 | solution.py:166
  186.5 3.8 %conditional.3 = ((f32[2,512]{1,0:T(2,128)S(1)}, f32[2,512]{1,0:T(2,128)S(1)}, f32[2,512,64]{1,2,0:T(8,128)S(1)})) conditional(s32[]{:T(128)} %convert_element_type.82, (f32[2,512]{1,0:T(2,128)S(1)}, f32[2,512]{1,0:T(2,128)S(1)}, f32[2,512,64]{1,2,0:T(8,128)S(1)}) %tuple.88, (s32[]{:T(128)}, s32[]{:T(128)}, bf16[16384,128]{0,1:T(8,128)(2,1)}, ...), branch_computations={%region_2.0_spmd, %region_3.5_spmd} | conditional | flops 140120064 | bytes 8875094 | solution.py:166
  190.4 3.8 %conditional.3 = ((f32[2,512]{1,0:T(2,128)S(1)}, f32[2,512]{1,0:T(2,128)S(1)}, f32[2,512,64]{1,2,0:T(8,128)S(1)})) conditional(s32[]{:T(128)} %convert_element_type.82, (f32[2,512]{1,0:T(2,128)S(1)}, f32[2,512]{1,0:T(2,128)S(1)}, f32[2,512,64]{1,2,0:T(8,128)S(1)}) %tuple.88, (s32[]{:T(128)}, s32[]{:T(128)}, bf16[16384,128]{0,1:T(8,128)(2,1)}, ...), branch_computations={%region_2.0_spmd, %region_3.5_spmd} | conditional | flops 140120064 | bytes 8875094 | solution.py:166
  194.2 3.8 %conditional.3 = ((f32[2,512]{1,0:T(2,128)S(1)}, f32[2,512]{1,0:T(2,128)S(1)}, f32[2,512,64]{1,2,0:T(8,128)S(1)})) conditional(s32[]{:T(128)} %convert_element_type.82, (f32[2,512]{1,0:T(2,128)S(1)}, f32[2,512]{1,0:T(2,128)S(1)}, f32[2,512,64]{1,2,0:T(8,128)S(1)}) %tuple.88, (s32[]{:T(128)}, s32[]{:T(128)}, bf16[16384,128]{0,1:T(8,128)(2,1)}, ...), branch_computations={%region_2.0_spmd, %region_3.5_spmd} | conditional | flops 140120064 | bytes 8875094 | solution.py:166
  198.1 3.8 %conditional.3 = ((f32[2,512]{1,0:T(2,128)S(1)}, f32[2,512]{1,0:T(2,128)S(1)}, f32[2,512,64]{1,2,0:T(8,128)S(1)})) conditional(s32[]{:T(128)} %convert_element_type.82, (f32[2,512]{1,0:T(2,128)S(1)}, f32[2,512]{1,0:T(2,128)S(1)}, f32[2,512,64]{1,2,0:T(8,128)S(1)}) %tuple.88, (s32[]{:T(128)}, s32[]{:T(128)}, bf16[16384,128]{0,1:T(8,128)(2,1)}, ...), branch_computations={%region_2.0_spmd, %region_3.5_spmd} | conditional | flops 140120064 | bytes 8875094 | solution.py:166
  202.0 3.8 %conditional.3 = ((f32[2,512]{1,0:T(2,128)S(1)}, f32[2,512]{1,0:T(2,128)S(1)}, f32[2,512,64]{1,2,0:T(8,128)S(1)})) conditional(s32[]{:T(128)} %convert_element_type.82, (f32[2,512]{1,0:T(2,128)S(1)}, f32[2,512]{1,0:T(2,128)S(1)}, f32[2,512,64]{1,2,0:T(8,128)S(1)}) %tuple.88, (s32[]{:T(128)}, s32[]{:T(128)}, bf16[16384,128]{0,1:T(8,128)(2,1)}, ...), branch_computations={%region_2.0_spmd, %region_3.5_spmd} | conditional | flops 140120064 | bytes 8875094 | solution.py:166
  205.9 3.8 %conditional.3 = ((f32[2,512]{1,0:T(2,128)S(1)}, f32[2,512]{1,0:T(2,128)S(1)}, f32[2,512,64]{1,2,0:T(8,128)S(1)})) conditional(s32[]{:T(128)} %convert_element_type.82, (f32[2,512]{1,0:T(2,128)S(1)}, f32[2,512]{1,0:T(2,128)S(1)}, f32[2,512,64]{1,2,0:T(8,128)S(1)}) %tuple.88, (s32[]{:T(128)}, s32[]{:T(128)}, bf16[16384,128]{0,1:T(8,128)(2,1)}, ...), branch_computations={%region_2.0_spmd, %region_3.5_spmd} | conditional | flops 140120064 | bytes 8875094 | solution.py:166
  209.7 3.8 %conditional.3 = ((f32[2,512]{1,0:T(2,128)S(1)}, f32[2,512]{1,0:T(2,128)S(1)}, f32[2,512,64]{1,2,0:T(8,128)S(1)})) conditional(s32[]{:T(128)} %convert_element_type.82, (f32[2,512]{1,0:T(2,128)S(1)}, f32[2,512]{1,0:T(2,128)S(1)}, f32[2,512,64]{1,2,0:T(8,128)S(1)}) %tuple.88, (s32[]{:T(128)}, s32[]{:T(128)}, bf16[16384,128]{0,1:T(8,128)(2,1)}, ...), branch_computations={%region_2.0_spmd, %region_3.5_spmd} | conditional | flops 140120064 | bytes 8875094 | solution.py:166
  213.6 3.8 %conditional.3 = ((f32[2,512]{1,0:T(2,128)S(1)}, f32[2,512]{1,0:T(2,128)S(1)}, f32[2,512,64]{1,2,0:T(8,128)S(1)})) conditional(s32[]{:T(128)} %convert_element_type.82, (f32[2,512]{1,0:T(2,128)S(1)}, f32[2,512]{1,0:T(2,128)S(1)}, f32[2,512,64]{1,2,0:T(8,128)S(1)}) %tuple.88, (s32[]{:T(128)}, s32[]{:T(128)}, bf16[16384,128]{0,1:T(8,128)(2,1)}, ...), branch_computations={%region_2.0_spmd, %region_3.5_spmd} | conditional | flops 140120064 | bytes 8875094 | solution.py:166
  217.5 3.8 %conditional.3 = ((f32[2,512]{1,0:T(2,128)S(1)}, f32[2,512]{1,0:T(2,128)S(1)}, f32[2,512,64]{1,2,0:T(8,128)S(1)})) conditional(s32[]{:T(128)} %convert_element_type.82, (f32[2,512]{1,0:T(2,128)S(1)}, f32[2,512]{1,0:T(2,128)S(1)}, f32[2,512,64]{1,2,0:T(8,128)S(1)}) %tuple.88, (s32[]{:T(128)}, s32[]{:T(128)}, bf16[16384,128]{0,1:T(8,128)(2,1)}, ...), branch_computations={%region_2.0_spmd, %region_3.5_spmd} | conditional | flops 140120064 | bytes 8875094 | solution.py:166
  221.3 3.8 %conditional.3 = ((f32[2,512]{1,0:T(2,128)S(1)}, f32[2,512]{1,0:T(2,128)S(1)}, f32[2,512,64]{1,2,0:T(8,128)S(1)})) conditional(s32[]{:T(128)} %convert_element_type.82, (f32[2,512]{1,0:T(2,128)S(1)}, f32[2,512]{1,0:T(2,128)S(1)}, f32[2,512,64]{1,2,0:T(8,128)S(1)}) %tuple.88, (s32[]{:T(128)}, s32[]{:T(128)}, bf16[16384,128]{0,1:T(8,128)(2,1)}, ...), branch_computations={%region_2.0_spmd, %region_3.5_spmd} | conditional | flops 140120064 | bytes 8875094 | solution.py:166
  225.2 3.8 %conditional.3 = ((f32[2,512]{1,0:T(2,128)S(1)}, f32[2,512]{1,0:T(2,128)S(1)}, f32[2,512,64]{1,2,0:T(8,128)S(1)})) conditional(s32[]{:T(128)} %convert_element_type.82, (f32[2,512]{1,0:T(2,128)S(1)}, f32[2,512]{1,0:T(2,128)S(1)}, f32[2,512,64]{1,2,0:T(8,128)S(1)}) %tuple.88, (s32[]{:T(128)}, s32[]{:T(128)}, bf16[16384,128]{0,1:T(8,128)(2,1)}, ...), branch_computations={%region_2.0_spmd, %region_3.5_spmd} | conditional | flops 140120064 | bytes 8875094 | solution.py:166
  229.1 3.8 %conditional.3 = ((f32[2,512]{1,0:T(2,128)S(1)}, f32[2,512]{1,0:T(2,128)S(1)}, f32[2,512,64]{1,2,0:T(8,128)S(1)})) conditional(s32[]{:T(128)} %convert_element_type.82, (f32[2,512]{1,0:T(2,128)S(1)}, f32[2,512]{1,0:T(2,128)S(1)}, f32[2,512,64]{1,2,0:T(8,128)S(1)}) %tuple.88, (s32[]{:T(128)}, s32[]{:T(128)}, bf16[16384,128]{0,1:T(8,128)(2,1)}, ...), branch_computations={%region_2.0_spmd, %region_3.5_spmd} | conditional | flops 140120064 | bytes 8875094 | solution.py:166
  233.0 3.8 %conditional.3 = ((f32[2,512]{1,0:T(2,128)S(1)}, f32[2,512]{1,0:T(2,128)S(1)}, f32[2,512,64]{1,2,0:T(8,128)S(1)})) conditional(s32[]{:T(128)} %convert_element_type.82, (f32[2,512]{1,0:T(2,128)S(1)}, f32[2,512]{1,0:T(2,128)S(1)}, f32[2,512,64]{1,2,0:T(8,128)S(1)}) %tuple.88, (s32[]{:T(128)}, s32[]{:T(128)}, bf16[16384,128]{0,1:T(8,128)(2,1)}, ...), branch_computations={%region_2.0_spmd, %region_3.5_spmd} | conditional | flops 140120064 | bytes 8875094 | solution.py:166
  236.8 3.8 %conditional.3 = ((f32[2,512]{1,0:T(2,128)S(1)}, f32[2,512]{1,0:T(2,128)S(1)}, f32[2,512,64]{1,2,0:T(8,128)S(1)})) conditional(s32[]{:T(128)} %convert_element_type.82, (f32[2,512]{1,0:T(2,128)S(1)}, f32[2,512]{1,0:T(2,128)S(1)}, f32[2,512,64]{1,2,0:T(8,128)S(1)}) %tuple.88, (s32[]{:T(128)}, s32[]{:T(128)}, bf16[16384,128]{0,1:T(8,128)(2,1)}, ...), branch_computations={%region_2.0_spmd, %region_3.5_spmd} | conditional | flops 140120064 | bytes 8875094 | solution.py:166
  240.7 3.8 %conditional.3 = ((f32[2,512]{1,0:T(2,128)S(1)}, f32[2,512]{1,0:T(2,128)S(1)}, f32[2,512,64]{1,2,0:T(8,128)S(1)})) conditional(s32[]{:T(128)} %convert_element_type.82, (f32[2,512]{1,0:T(2,128)S(1)}, f32[2,512]{1,0:T(2,128)S(1)}, f32[2,512,64]{1,2,0:T(8,128)S(1)}) %tuple.88, (s32[]{:T(128)}, s32[]{:T(128)}, bf16[16384,128]{0,1:T(8,128)(2,1)}, ...), branch_computations={%region_2.0_spmd, %region_3.5_spmd} | conditional | flops 140120064 | bytes 8875094 | solution.py:166
  244.6 3.8 %conditional.3 = ((f32[2,512]{1,0:T(2,128)S(1)}, f32[2,512]{1,0:T(2,128)S(1)}, f32[2,512,64]{1,2,0:T(8,128)S(1)})) conditional(s32[]{:T(128)} %convert_element_type.82, (f32[2,512]{1,0:T(2,128)S(1)}, f32[2,512]{1,0:T(2,128)S(1)}, f32[2,512,64]{1,2,0:T(8,128)S(1)}) %tuple.88, (s32[]{:T(128)}, s32[]{:T(128)}, bf16[16384,128]{0,1:T(8,128)(2,1)}, ...), branch_computations={%region_2.0_spmd, %region_3.5_spmd} | conditional | flops 140120064 | bytes 8875094 | solution.py:166
  248.5 3.8 %conditional.3 = ((f32[2,512]{1,0:T(2,128)S(1)}, f32[2,512]{1,0:T(2,128)S(1)}, f32[2,512,64]{1,2,0:T(8,128)S(1)})) conditional(s32[]{:T(128)} %convert_element_type.82, (f32[2,512]{1,0:T(2,128)S(1)}, f32[2,512]{1,0:T(2,128)S(1)}, f32[2,512,64]{1,2,0:T(8,128)S(1)}) %tuple.88, (s32[]{:T(128)}, s32[]{:T(128)}, bf16[16384,128]{0,1:T(8,128)(2,1)}, ...), branch_computations={%region_2.0_spmd, %region_3.5_spmd} | conditional | flops 140120064 | bytes 8875094 | solution.py:166
  252.3 3.8 %conditional.3 = ((f32[2,512]{1,0:T(2,128)S(1)}, f32[2,512]{1,0:T(2,128)S(1)}, f32[2,512,64]{1,2,0:T(8,128)S(1)})) conditional(s32[]{:T(128)} %convert_element_type.82, (f32[2,512]{1,0:T(2,128)S(1)}, f32[2,512]{1,0:T(2,128)S(1)}, f32[2,512,64]{1,2,0:T(8,128)S(1)}) %tuple.88, (s32[]{:T(128)}, s32[]{:T(128)}, bf16[16384,128]{0,1:T(8,128)(2,1)}, ...), branch_computations={%region_2.0_spmd, %region_3.5_spmd} | conditional | flops 140120064 | bytes 8875094 | solution.py:166
  256.2 3.8 %conditional.3 = ((f32[2,512]{1,0:T(2,128)S(1)}, f32[2,512]{1,0:T(2,128)S(1)}, f32[2,512,64]{1,2,0:T(8,128)S(1)})) conditional(s32[]{:T(128)} %convert_element_type.82, (f32[2,512]{1,0:T(2,128)S(1)}, f32[2,512]{1,0:T(2,128)S(1)}, f32[2,512,64]{1,2,0:T(8,128)S(1)}) %tuple.88, (s32[]{:T(128)}, s32[]{:T(128)}, bf16[16384,128]{0,1:T(8,128)(2,1)}, ...), branch_computations={%region_2.0_spmd, %region_3.5_spmd} | conditional | flops 140120064 | bytes 8875094 | solution.py:166
  260.1 3.8 %conditional.3 = ((f32[2,512]{1,0:T(2,128)S(1)}, f32[2,512]{1,0:T(2,128)S(1)}, f32[2,512,64]{1,2,0:T(8,128)S(1)})) conditional(s32[]{:T(128)} %convert_element_type.82, (f32[2,512]{1,0:T(2,128)S(1)}, f32[2,512]{1,0:T(2,128)S(1)}, f32[2,512,64]{1,2,0:T(8,128)S(1)}) %tuple.88, (s32[]{:T(128)}, s32[]{:T(128)}, bf16[16384,128]{0,1:T(8,128)(2,1)}, ...), branch_computations={%region_2.0_spmd, %region_3.5_spmd} | conditional | flops 140120064 | bytes 8875094 | solution.py:166
  264.0 3.8 %conditional.3 = ((f32[2,512]{1,0:T(2,128)S(1)}, f32[2,512]{1,0:T(2,128)S(1)}, f32[2,512,64]{1,2,0:T(8,128)S(1)})) conditional(s32[]{:T(128)} %convert_element_type.82, (f32[2,512]{1,0:T(2,128)S(1)}, f32[2,512]{1,0:T(2,128)S(1)}, f32[2,512,64]{1,2,0:T(8,128)S(1)}) %tuple.88, (s32[]{:T(128)}, s32[]{:T(128)}, bf16[16384,128]{0,1:T(8,128)(2,1)}, ...), branch_computations={%region_2.0_spmd, %region_3.5_spmd} | conditional | flops 140120064 | bytes 8875094 | solution.py:166
  267.8 3.8 %conditional.3 = ((f32[2,512]{1,0:T(2,128)S(1)}, f32[2,512]{1,0:T(2,128)S(1)}, f32[2,512,64]{1,2,0:T(8,128)S(1)})) conditional(s32[]{:T(128)} %convert_element_type.82, (f32[2,512]{1,0:T(2,128)S(1)}, f32[2,512]{1,0:T(2,128)S(1)}, f32[2,512,64]{1,2,0:T(8,128)S(1)}) %tuple.88, (s32[]{:T(128)}, s32[]{:T(128)}, bf16[16384,128]{0,1:T(8,128)(2,1)}, ...), branch_computations={%region_2.0_spmd, %region_3.5_spmd} | conditional | flops 140120064 | bytes 8875094 | solution.py:166
  271.7 3.8 %conditional.3 = ((f32[2,512]{1,0:T(2,128)S(1)}, f32[2,512]{1,0:T(2,128)S(1)}, f32[2,512,64]{1,2,0:T(8,128)S(1)})) conditional(s32[]{:T(128)} %convert_element_type.82, (f32[2,512]{1,0:T(2,128)S(1)}, f32[2,512]{1,0:T(2,128)S(1)}, f32[2,512,64]{1,2,0:T(8,128)S(1)}) %tuple.88, (s32[]{:T(128)}, s32[]{:T(128)}, bf16[16384,128]{0,1:T(8,128)(2,1)}, ...), branch_computations={%region_2.0_spmd, %region_3.5_spmd} | conditional | flops 140120064 | bytes 8875094 | solution.py:166
  275.6 4.2 %add_convert_fusion = bf16[512,2048]{1,0:T(8,128)(2,1)} fusion(f32[512,2048]{1,0:T(8,128)} %fusion.46, bf16[512,128]{0,1:T(8,128)(2,1)S(1)} %bitcast.65, bf16[128,2048]{1,0:T(8,128)(2,1)S(1)} %copy-done.4), kind=kOutput, calls=%fused_computation.22 | convolution fusion | flops 270532608 | bytes 6946816 | tf_op jit(solution)/shard_map/dot_general | solution.py:195
  279.8 4.3 %all-to-all-start.2 = ((bf16[8,64,2048]{2,1,0:T(8,128)(2,1)}), bf16[8,64,2048]{2,1,0:T(8,128)(2,1)S(1)}, u32[]{:S(2)}, u32[]{:S(2)}) async-start(bf16[8,64,2048]{2,1,0:T(8,128)(2,1)} %bitcast.63), calls=%async_computation.2 | async-start | bytes 4194304 | tf_op jit(solution)/shard_map/all_to_all | solution.py:54
  284.7 26.6 %all-to-all-done.2 = bf16[8,64,2048]{2,1,0:T(8,128)(2,1)S(1)} async-done(((bf16[8,64,2048]{2,1,0:T(8,128)(2,1)}), bf16[8,64,2048]{2,1,0:T(8,128)(2,1)S(1)}, u32[]{:S(2)}, u32[]{:S(2)}) %all-to-all-start.2) | async-done | bytes 2097184 | tf_op jit(solution)/shard_map/all_to_all | solution.py:54
  (428 shorter events, 131.0 us)
Async XLA Ops:
  7.2 61.7 %copy-start = (bf16[256,2048]{1,0:T(8,128)(2,1)S(1)}, bf16[256,2048]{1,0:T(8,128)(2,1)}, u32[]{:S(2)}) copy-start(bf16[256,2048]{1,0:T(8,128)(2,1)} %param.27) | copy-start | bytes 3145732
  7.2 138.4 %all-gather.2.cloned.1.call-start = ((), (), s32[]{:S(2)}) async-start(), calls=%async_computation.3 | async-start | bytes 8650752 | tf_op jit(solution)/shard_map/all_gather | solution.py:29
  40.0 1.3 copy-start.1
  41.3 0.7 copy-start.6
  42.0 2.2 copy-start.2
  44.2 1.0 copy-start.3
  45.3 1.6 copy-start.5
  47.5 2.0 copy-start.9
  50.3 5.6 %collective-permute-start = (bf16[30,256]{1,0:T(8,128)(2,1)S(1)}, bf16[30,256]{1,0:T(8,128)(2,1)S(1)}, u32[]{:S(2)}, u32[]{:S(2)}) collective-permute-start(bf16[30,256]{1,0:T(8,128)(2,1)S(1)} %slice.262), channel_id=1, source_target_pairs={{0,8},{8,16},{16,24},{24,32},{32,40},{40,48},{48,56},{56,64},{64,7... | collective-permute-start | bytes 46088 | tf_op jit(solution)/shard_map/ppermute | solution.py:39
  59.6 9.3 %copy-start.8 = (f32[256]{0:T(256)S(1)}, f32[256]{0:T(256)}, u32[]{:S(2)}) copy-start(f32[256]{0:T(256)} %param.24) | copy-start | bytes 3076
  60.2 8.6 %all-to-all-start.1 = ((f32[8,1,512]{2,1,0:T(1,128)}), f32[8,1,512]{2,1,0:T(1,128)S(1)}, u32[]{:S(2)}, u32[]{:S(2)}) async-start(f32[8,1,512]{2,1,0:T(1,128)} %broadcast_in_dim.66), calls=%async_computation.1 | async-start | bytes 32768 | tf_op jit(solution)/shard_map/all_to_all | solution.py:11
  72.7 78.9 %copy-start.7 = (f32[2,512]{1,0:T(2,128)S(1)}, f32[2,512]{1,0:T(2,128)}, u32[]{:S(2)}) copy-start(f32[2,512]{1,0:T(2,128)} %constant_dynamic-slice_fusion.3) | copy-start | bytes 12292
  151.5 124.1 %copy-start.4 = (bf16[128,2048]{1,0:T(8,128)(2,1)S(1)}, bf16[128,2048]{1,0:T(8,128)(2,1)}, u32[]{:S(2)}) copy-start(bf16[128,2048]{1,0:T(8,128)(2,1)} %param.26) | copy-start | bytes 1572868
  279.8 31.4 %all-to-all-start.2 = ((bf16[8,64,2048]{2,1,0:T(8,128)(2,1)}), bf16[8,64,2048]{2,1,0:T(8,128)(2,1)S(1)}, u32[]{:S(2)}, u32[]{:S(2)}) async-start(bf16[8,64,2048]{2,1,0:T(8,128)(2,1)} %bitcast.63), calls=%async_computation.2 | async-start | bytes 4194304 | tf_op jit(solution)/shard_map/all_to_all | solution.py:54
Sparse Core Ops, SparseCore 0:
  47.0 98.5 all-gather.1
where the time goes:
time: 321 us; the launch traced here: 319 us
  waiting for transfers between devices  106 us (33%)
  local copies, waits for them, and re-layouts  65.4 us (20%)
  matrix products  57.7 us (18%)
  blocking collectives  31.5 us (10%)
  other arithmetic  31.4 us (10%)
  between operations  14.2 us (4%)
  starting transfers between devices  8.93 us (3%)
  loops' own time  4.04 us (1%)
    all_gather x1, waiting for transfers between devices, sent_together(): result, at, done = (lax.all_gather(both, axis, axis=dim, tiled=True), 0, [])  73 us
    dynamic_slice x32, local copies, waits for them, and re-layouts, advance(): lax.dynamic_slice_in_dim(value_group, begin_row, local_rows, 0)  31.5 us
    all_to_all x1, blocking collectives, from_everyone(): lax.all_to_all(jnp.broadcast_to(array[None], (length, *array.shape)), axi...  31.5 us
    all_to_all x1, waiting for transfers between devices, sent_and_summed(): lax.all_to_all(split_up(array, dim, length), axis, 0, 0, tiled=True)  26.6 us
    dot_general x32, matrix products, absorb(): jnp.einsum('qhd,khd->hqk', query_heads, key_heads, preferred_element_type...  22.7 us
    dynamic_slice x32, local copies, waits for them, and re-layouts, absorb(): cum_keys = lax.dynamic_slice_in_dim(cum_gate, first_place, length_in, 1)  22.3 us
    dot_general x32, matrix products, absorb(): jnp.einsum('hqk,khd->hqd', weights.astype(jnp.bfloat16), value_heads, pre...  20.8 us
    reduce_sum x32, other arithmetic, absorb(): row_total = shrink * row_total + jnp.sum(weights, axis=2)  13.7 us
  transfers between devices with their start and end apart: 4, of which 4 were waited for; matrix products, arithmetic and copies ran while one was open for 5% of the time, Pallas kernels for 0%

commit v1 on v0

v1 whole, which is shorter than its diff:
```python
import functools

import jax
import jax.numpy as jnp
from jax import lax
from jax.experimental import pallas as pl
from jax.experimental.pallas import tpu as pltpu
from jax.sharding import PartitionSpec as P

MESH = pl.DeviceIdType.MESH
F32 = jnp.float32
BF16 = jnp.bfloat16
HEAD = 64
NX = 4
NY = 4
LOW = -1e30
LOG2E = 1.4426950408889634
VROWS = 80


def kernel(
    tokens,
    norm_gain,
    w_query,
    w_key,
    w_value,
    conv_in,
    conv_gate,
    conv_taps,
    conv_gain,
    cum_gate,
    out_attn,
    out_conv,
    mixed,
    log_total,
    nt,
    wall,
    wout,
    qp,
    ks,
    vs,
    kp,
    vp,
    cpad,
    mrow,
    acc,
    obuf,
    orecv,
    sbuf,
    srecv,
    gb,
    rim,
    cg,
    cv,
    sq,
    csq,
    xs,
    sb,
    rb,
    po,
    t2,
    r2r,
    r2l,
    sr,
    sl,
    frl,
    frr,
    wsem,
    gsend,
    grecv,
    ksend,
    krecv,
    vsend,
    vrecv,
    qsend,
    qrecv,
    msend,
    mrecv,
    osend,
    orecv_sem,
    csend,
    crecv,
    xsend,
    xrecv,
):
    s_me = lax.axis_index("sp")
    t_me = lax.axis_index("tp")
    nsp = lax.axis_size("sp")
    nz = nsp // NX
    z = s_me // NX
    x = s_me % NX
    y = t_me // 2
    c = t_me % 2
    rows = tokens.shape[0]
    half = rows // 2
    depth = tokens.shape[1]
    tok = rows * 8

    def at_tp(t):
        return (s_me, t)

    def at_sp(s):
        return (s, t_me)

    def rcopy(src, dst, ssem, rsem, dev):
        return pltpu.make_async_remote_copy(
            src_ref=src,
            dst_ref=dst,
            send_sem=ssem,
            recv_sem=rsem,
            device_id=dev,
            device_id_type=MESH,
        )

    wcopies = []
    at = 0
    for i, w in enumerate((w_query, w_key, w_value, conv_in, conv_gate)):
        n = w.shape[1]
        wcopies.append(pltpu.make_async_copy(w, wall.at[:, pl.ds(at, n)], wsem.at[i]))
        at += n
    at = 0
    ocopies = []
    for i, w in enumerate((out_attn, out_conv)):
        n = w.shape[0]
        ocopies.append(pltpu.make_async_copy(w, wout.at[pl.ds(at, n), :], wsem.at[5 + i]))
        at += n
    for w in wcopies + ocopies:
        w.start()

    barrier = pltpu.get_barrier_semaphore()
    for d in range(1, 8):
        pl.semaphore_signal(
            barrier, inc=1, device_id=at_tp((t_me + d) % 8), device_id_type=MESH
        )
    for d in range(1, NX):
        pl.semaphore_signal(
            barrier, inc=1, device_id=at_sp(z * NX + (x + d) % NX), device_id_type=MESH
        )
    for d in (1, nz - 1):
        pl.semaphore_signal(
            barrier, inc=1, device_id=at_sp(((z + d) % nz) * NX + x), device_id_type=MESH
        )
    for d in (1, nsp - 1):
        pl.semaphore_signal(
            barrier, inc=1, device_id=at_sp((s_me + d) % nsp), device_id_type=MESH
        )

    wide = tokens[...].astype(F32)
    factor = lax.rsqrt(jnp.mean(wide * wide, axis=1, keepdims=True) + 1e-06)
    nt[t_me] = (wide * factor * norm_gain[...]).astype(BF16)
    qp[:, 0, HEAD:, :] = jnp.ones((NX, HEAD, tok), BF16)
    qp[:, 1, :HEAD, :] = jnp.ones((NX, HEAD, tok), BF16)
    vp[:, HEAD:, :] = jnp.ones((2, VROWS - HEAD, tok), BF16)
    cpad[...] = jnp.zeros_like(cpad)
    mrow[...] = jnp.full_like(mrow, LOW)
    acc[...] = jnp.zeros_like(acc)

    pl.semaphore_wait(barrier, 7 + NX - 1 + 4)

    sib = y * 2 + (1 - c)
    tr = ((y + 1) % NY) * 2 + c
    tl = ((y + NY - 1) % NY) * 2 + c
    to = ((y + 2) % NY) * 2 + c
    lo, hi = pl.ds(0, half), pl.ds(half, half)

    def gcopy(k, src, part, dev):
        ref = nt.at[src] if part is None else nt.at[src, part]
        return rcopy(ref, ref, gsend.at[k], grecv.at[k], at_tp(dev))

    g = [
        gcopy(0, t_me, None, sib),
        gcopy(1, t_me, lo, tr),
        gcopy(2, t_me, hi, tr),
        gcopy(3, t_me, hi, tl),
        gcopy(4, t_me, lo, tl),
        gcopy(5, tl, None, sib),
        gcopy(6, tr, None, sib),
        gcopy(7, tl, lo, tr),
        gcopy(8, tr, hi, tl),
        gcopy(9, to, lo, sib),
        gcopy(10, to, hi, sib),
    ]
    for k in (1, 3, 2, 4, 0):
        g[k].start()
    for w in wcopies:
        w.wait()

    def project(i, carry):
        @pl.when(i == 0)
        def _():
            g[0].wait_recv()

        @pl.when(i == 1)
        def _():
            g[1].wait_recv()
            g[7].start()
            g[3].wait_recv()
            g[8].start()
            g[2].wait_recv()
            g[5].start()
            g[4].wait_recv()
            g[6].start()
            g[5].wait_recv()

        @pl.when(i == 2)
        def _():
            g[6].wait_recv()

        @pl.when(i == 3)
        def _():
            g[7].wait_recv()
            g[9].start()
            g[8].wait_recv()
            g[10].start()
            g[9].wait_recv()
            g[10].wait_recv()

        p = (y + 2 * NY - (2 * (i % 2) - 1) * ((i + 1) // 2)) % NY
        lhs = nt[pl.ds(2 * p, 2)].reshape(2 * rows, depth)
        res = jnp.dot(lhs, wall[...], preferred_element_type=F32)
        here = pl.ds(pl.multiple_of(p * 2 * rows, 2 * rows), 2 * rows)
        qt = (res[:, :128] * HEAD ** (-0.5)).T.astype(BF16)
        qp[x, 0, :HEAD, here] = qt[:HEAD]
        qp[x, 1, HEAD:, here] = qt[HEAD:]
        ks[z, here, :] = res[:, 128:256].astype(BF16)
        vs[z, :, here] = res[:, 256:384].T.astype(BF16)
        opened = res[:, 384:640]
        gating = res[:, 640:896]
        gate = (opened / (1.0 + jnp.exp(-gating))).astype(BF16)
        gb[here, :] = gate
        cg[pl.ds(pl.multiple_of(p * 2 * rows + 32, 32), 2 * rows), :] = gate.astype(F32)
        return carry

    lax.fori_loop(0, NY, project, 0)

    def sp_of(zz):
        return at_sp(zz * NX + x)

    def kcopy(zb, t, zt):
        return rcopy(ks.at[zb], ks.at[zb], ksend.at[t], krecv.at[t], sp_of(zt))

    def vcopy(zb, t, zt):
        return rcopy(vs.at[zb], vs.at[zb], vsend.at[t], vrecv.at[t], sp_of(zt))

    for t, zt in ((1, (z + 1) % nz), (2, (z + nz - 1) % nz)):
        kcopy(z, t, zt).start()
        vcopy(z, t, zt).start()

    def qcopies(src, d):
        dev = at_sp(z * NX + (x + d) % NX)
        a = qp.at[src, 0, pl.ds(0, HEAD)]
        b = qp.at[src, 1, pl.ds(HEAD, HEAD)]
        return (
            rcopy(a, a, qsend.at[2 * d - 2], qrecv.at[2 * d - 2], dev),
            rcopy(b, b, qsend.at[2 * d - 1], qrecv.at[2 * d - 1], dev),
        )

    for d in (1, 3, 2):
        for q in qcopies(x, d):
            q.start()
    rcopy_rim = rcopy(
        gb.at[pl.ds(tok - 32, 32)], rim, msend.at[0], mrecv.at[0], at_sp((s_me + 1) % nsp)
    )
    rcopy_rim.start()

    rcopy_rim.wait_recv()
    first = jnp.where(s_me > 0, 1.0, 0.0).astype(F32)
    cg[0:32, :] = rim[...].astype(F32) * first

    def conv_rows(i, carry):
        r0 = pl.multiple_of(i * 64, 64)
        win = cg[pl.ds(r0, 96), :]
        total = jnp.zeros((64, win.shape[1]), F32)
        for b in range(8):
            turned = win if b == 0 else pltpu.roll(win, 96 - b, 0)
            for a in range(5):
                k = 8 * a + b - 2
                if 0 <= k < 31:
                    total = total + conv_taps[k : k + 1, :] * turned[8 * a : 8 * a + 64]
        cv[pl.ds(r0, 64), :] = total
        square = total * total
        sq[pl.ds(r0, 64), :] = square[:, :128] + square[:, 128:]
        return carry

    lax.fori_loop(0, tok // 64, conv_rows, 0)
    part = jnp.sum(sq[...].T, axis=0, keepdims=True)
    csq[t_me] = jnp.broadcast_to(part, (8, tok))
    ccopies = []
    for d in range(1, 8):
        cc = rcopy(
            csq.at[t_me], csq.at[t_me], csend.at[d], crecv.at[d], at_tp((t_me + d) % 8)
        )
        cc.start()
        ccopies.append(cc)

    cref = cum_gate[:, pl.ds(pl.multiple_of(z * NX * tok, 128), 128)][:, :1]

    def prepare(zb):
        ck = cum_gate[:, pl.ds(pl.multiple_of((zb * NX + x) * tok, 128), tok)]
        bias = cref - ck
        high = bias.astype(BF16).astype(F32)
        left = bias - high
        mid = left.astype(BF16).astype(F32)
        low = left - mid
        rowid = lax.broadcasted_iota(jnp.int32, (8, tok), 0)
        for h, r0 in ((0, HEAD), (1, 0)):
            tile = jnp.where(
                rowid == 0,
                high[h : h + 1],
                jnp.where(
                    rowid == 1, mid[h : h + 1], jnp.where(rowid == 2, low[h : h + 1], 0.0)
                ),
            )
            cpad[r0 : r0 + 8, :] = tile
        extra = cpad[...].T
        kf = ks[zb].astype(F32)
        lane = lax.broadcasted_iota(jnp.int32, (tok, 2 * HEAD), 1)
        kp[0] = jnp.where(lane < HEAD, kf, extra).astype(BF16)
        kp[1] = jnp.where(lane < HEAD, extra, kf).astype(BF16)
        vp[0, :HEAD, :] = vs[zb, :HEAD, :]
        vp[1, :HEAD, :] = vs[zb, HEAD:, :]

    def chunk(j, masked):
        for h in range(2):
            sc = jnp.dot(kp[h], qp[j, h], preferred_element_type=F32)
            if masked:
                kpos = lax.broadcasted_iota(jnp.int32, sc.shape, 0)
                qpos = lax.broadcasted_iota(jnp.int32, sc.shape, 1)
                sc = jnp.where(kpos <= qpos, sc, LOW)
            old = mrow[j, h]
            new = jnp.maximum(old, jnp.max(sc, axis=0, keepdims=True))
            wts = jnp.exp2((sc - new) * LOG2E).astype(BF16)
            shrink = jnp.exp2((old - new) * LOG2E)
            mrow[j, h] = new
            acc[j, h] = acc[j, h] * shrink + jnp.dot(vp[h], wts, preferred_element_type=F32)

    def full(j, carry):
        chunk(j, False)
        return carry

    prepare(z)
    chunk(x, True)
    for d in range(1, NX):
        for q in qcopies((x + NX - d) % NX, d):
            q.wait_recv()
    lax.fori_loop(x + 1, NX, full, 0)

    def arrival(t, carry):
        dr = 2 * (t % 2) - 1
        zb = (z + nz - dr * ((t + 1) // 2)) % nz
        zt = (z + nz + dr) % nz
        kcopy(zb, t, zt).wait_recv()

        @pl.when(t <= 5)
        def _():
            kcopy(zb, t + 2, zt).start()

        vcopy(zb, t, zt).wait_recv()

        @pl.when((t <= 4) | (t == 6))
        def _():
            vcopy(zb, t + 2 - t // 6, zt).start()

        @pl.when(zb < z)
        def _():
            prepare(zb)
            lax.fori_loop(0, NX, full, 0)

        return carry

    lax.fori_loop(1, nz, arrival, 0)

    xcopies = []
    for d in (1, 3, 2):
        j = (x + d) % NX
        for h in range(2):
            obuf[d - 1, h * HEAD : (h + 1) * HEAD, :] = acc[j, h, :HEAD, :].astype(BF16)
            sbuf[d - 1, h : h + 1, :] = mrow[j, h]
            sbuf[d - 1, 2 + h : 3 + h, :] = acc[j, h, HEAD : HEAD + 1, :]
        dev = at_sp(z * NX + j)
        oc = rcopy(
            obuf.at[d - 1], orecv.at[d - 1], osend.at[2 * d - 2], orecv_sem.at[2 * d - 2], dev
        )
        st = rcopy(
            sbuf.at[d - 1], srecv.at[d - 1], osend.at[2 * d - 1], orecv_sem.at[2 * d - 1], dev
        )
        st.start()
        oc.start()
        xcopies += [oc, st]

    for cc in ccopies:
        cc.wait_recv()
    total = csq[0, 0:1, :]
    for t in range(1, 8):
        total = total + csq[t, 0:1, :]
    scale = lax.rsqrt(total / (8.0 * conv_gain.shape[1]) + 1e-06)
    sq[...] = jnp.broadcast_to(scale, (128, tok)).T
    for i in range(8):
        r = pl.ds(i * rows, rows)
        factor = sq[r, :]
        for b in range(2):
            lanes = pl.ds(b * 128, 128)
            v = cv[r, lanes] * factor * conv_gain[:, lanes]
            v = v / (1.0 + jnp.exp(-v))
            xs[i % 2, i // 2, :, pl.ds(128 + b * 128, 128)] = v.astype(BF16)
    for w in ocopies:
        w.wait()

    for cp in xcopies:
        cp.wait_recv()
    offset = pl.multiple_of(s_me * tok, 128)
    for h in range(2):
        best = mrow[x, h]
        for d in range(1, NX):
            best = jnp.maximum(best, srecv[d - 1, h : h + 1, :])
        share = jnp.exp2((mrow[x, h] - best) * LOG2E)
        summed = acc[x, h, HEAD : HEAD + 1, :] * share
        value = acc[x, h, :HEAD, :] * share
        for d in range(1, NX):
            share = jnp.exp2((srecv[d - 1, h : h + 1, :] - best) * LOG2E)
            summed = summed + srecv[d - 1, 2 + h : 3 + h, :] * share
            value = value + orecv[d - 1, h * HEAD : (h + 1) * HEAD, :].astype(F32) * share
        own = cum_gate[:, pl.ds(offset, tok)][h : h + 1] - cref[h : h + 1]
        log_total[h : h + 1, :] = best + jnp.log(summed) + own
        cpad[h * HEAD : (h + 1) * HEAD, :] = value / summed
    att = cpad[...].T.astype(BF16)
    for i in range(8):
        xs[i % 2, i // 2, :, 0:128] = att[i * rows : (i + 1) * rows]

    def project_out(which, emit):
        lhs = xs[which].reshape(NY * rows, 384)

        def columns(n, carry):
            cols = pl.ds(pl.multiple_of(n * 512, 512), 512)
            res = jnp.dot(lhs, wout[:, cols], preferred_element_type=F32)
            emit(cols, res)
            return carry

        lax.fori_loop(0, depth // 512, columns, 0)

    def emit_sib(cols, res):
        sb[:, :, cols] = res.astype(BF16).reshape(NY, rows, 512)

    def emit_own(cols, res):
        po[:, :, cols] = res.reshape(NY, rows, 512)

    project_out(1 - c, emit_sib)
    ybits = [(y + k) % NY for k in range(NY)]

    def xcopy(k, src, dst, dev):
        return rcopy(src, dst, xsend.at[k], xrecv.at[k], at_tp(dev))

    bcopies = [xcopy(k, sb.at[ybits[k]], rb.at[ybits[k]], sib) for k in range(NY)]
    for k in (2, 1, 3, 0):
        bcopies[k].start()
    project_out(c, emit_own)

    bcopies[2].wait_recv()
    t2[...] = (po[ybits[2]] + rb[ybits[2]].astype(F32)).astype(BF16)
    far_r = xcopy(4, t2.at[lo], r2r, tr)
    far_l = xcopy(5, t2.at[hi], r2l, tl)
    far_r.start()
    far_l.start()
    bcopies[1].wait_recv()
    sr[hi, :] = (po[ybits[1], hi] + rb[ybits[1], hi].astype(F32)).astype(BF16)
    near_r = xcopy(6, sr.at[hi], frl.at[hi], tr)
    near_r.start()
    bcopies[3].wait_recv()
    sl[lo, :] = (po[ybits[3], lo] + rb[ybits[3], lo].astype(F32)).astype(BF16)
    near_l = xcopy(7, sl.at[lo], frr.at[lo], tl)
    near_l.start()
    far_r.wait_recv()
    sr[lo, :] = (po[ybits[1], lo] + rb[ybits[1], lo].astype(F32) + r2r[...].astype(F32)).astype(BF16)
    both_r = xcopy(8, sr.at[lo], frl.at[lo], tr)
    both_r.start()
    far_l.wait_recv()
    sl[hi, :] = (po[ybits[3], hi] + rb[ybits[3], hi].astype(F32) + r2l[...].astype(F32)).astype(BF16)
    both_l = xcopy(9, sl.at[hi], frr.at[hi], tl)
    both_l.start()
    bcopies[0].wait_recv()
    po[ybits[0]] = po[ybits[0]] + rb[ybits[0]].astype(F32)
    near_r.wait_recv()
    near_l.wait_recv()
    both_r.wait_recv()
    both_l.wait_recv()
    mixed[...] = (po[y] + frl[...].astype(F32) + frr[...].astype(F32)).astype(BF16)

    for cp in g:
        cp.wait_send()
    for t in range(1, 8):
        kcopy(z, t, (z + 1) % nz).wait_send()
        vcopy(z, t, (z + 1) % nz).wait_send()
    for d in range(1, NX):
        for q in qcopies(x, d):
            q.wait_send()
    rcopy_rim.wait_send()
    for cp in ccopies + xcopies + bcopies:
        cp.wait_send()
    for cp in (far_r, far_l, near_r, near_l, both_r, both_l):
        cp.wait_send()


def per_device(*args):
    tokens = args[0]
    rows, depth = tokens.shape
    tok = rows * 8
    nz = lax.axis_size("sp") // NX
    att = args[2].shape[1]
    ch = args[5].shape[1]
    wide = 3 * att + 2 * ch
    ops = list(args)
    ops[1] = args[1][None]
    ops[8] = args[8][None]
    vmem = pl.BlockSpec(memory_space=pltpu.VMEM)
    hbm = pl.BlockSpec(memory_space=pltpu.HBM)
    specs = [vmem, vmem, hbm, hbm, hbm, hbm, hbm, vmem, vmem, vmem, hbm, hbm]
    dma = pltpu.SemaphoreType.DMA
    scratch = [
        pltpu.VMEM((8, rows, depth), BF16),
        pltpu.VMEM((depth, wide), BF16),
        pltpu.VMEM((att + ch, depth), BF16),
        pltpu.VMEM((NX, 2, att, tok), BF16),
        pltpu.VMEM((nz, tok, att), BF16),
        pltpu.VMEM((nz, att, tok), BF16),
        pltpu.VMEM((2, tok, att), BF16),
        pltpu.VMEM((2, VROWS, tok), BF16),
        pltpu.VMEM((att, tok), F32),
        pltpu.VMEM((NX, 2, 1, tok), F32),
        pltpu.VMEM((NX, 2, VROWS, tok), F32),
        pltpu.VMEM((NX - 1, att, tok), BF16),
        pltpu.VMEM((NX - 1, att, tok), BF16),
        pltpu.VMEM((NX - 1, 8, tok), F32),
        pltpu.VMEM((NX - 1, 8, tok), F32),
        pltpu.VMEM((tok, ch), BF16),
        pltpu.VMEM((32, ch), BF16),
        pltpu.VMEM((tok + 32, ch), F32),
        pltpu.VMEM((tok, ch), F32),
        pltpu.VMEM((tok, 128), F32),
        pltpu.VMEM((8, 8, tok), F32),
        pltpu.VMEM((2, NY, rows, att + ch), BF16),
        pltpu.VMEM((NY, rows, depth), BF16),
        pltpu.VMEM((NY, rows, depth), BF16),
        pltpu.VMEM((NY, rows, depth), F32),
        pltpu.VMEM((rows, depth), BF16),
        pltpu.VMEM((rows // 2, depth), BF16),
        pltpu.VMEM((rows // 2, depth), BF16),
        pltpu.VMEM((rows, depth), BF16),
        pltpu.VMEM((rows, depth), BF16),
        pltpu.VMEM((rows, depth), BF16),
        pltpu.VMEM((rows, depth), BF16),
        dma((7,)),
        dma((11,)),
        dma((11,)),
        dma((8,)),
        dma((8,)),
        dma((8,)),
        dma((8,)),
        dma((6,)),
        dma((6,)),
        dma((1,)),
        dma((1,)),
        dma((6,)),
        dma((6,)),
        dma((8,)),
        dma((8,)),
        dma((10,)),
        dma((10,)),
    ]
    return pl.pallas_call(
        kernel,
        out_shape=(
            jax.ShapeDtypeStruct((rows, depth), BF16),
            jax.ShapeDtypeStruct((2, tok), F32),
        ),
        in_specs=specs,
        out_specs=(vmem, vmem),
        scratch_shapes=scratch,
        compiler_params=pltpu.CompilerParams(
            collective_id=0, has_side_effects=True, vmem_limit_bytes=60 * 1024 * 1024
        ),
        name="layer",
    )(*ops)


def solution(mesh):
    in_specs = (
        P(("sp", "tp"), None),
        P(),
        P(None, "tp"),
        P(None, "tp"),
        P(None, "tp"),
        P(None, "tp"),
        P(None, "tp"),
        P(None, "tp"),
        P("tp"),
        P("tp", None),
        P("tp", None),
        P("tp", None),
    )
    out_specs = (P(("sp", "tp"), None), P("tp", "sp"))
    return jax.shard_map(
        per_device, mesh=mesh, in_specs=in_specs, out_specs=out_specs, check_vma=False
    )
```

time: 321 us -> 91.2 us (0.28)
  the two profiles are of different devices: /device:TPU:230 before, /device:TPU:228 now
where the time goes in v1:
time: 91.2 us; the launch traced here: 91.1 us
  Pallas kernels  88.2 us (97%)
  local copies, waits for them, and re-layouts  2.27 us (2%)
    pallas_call x1, Pallas kernels, per_device(): pl.pallas_call(kernel, out_shape=(jax.ShapeDtypeStruct((rows, depth), BF1...  88.2 us
    unnamed x4, local copies, waits for them, and re-layouts  2.27 us

profile of v1, /device:TPU:228, one launch (start us, length us, event | category | flops | bytes accessed | tf_op | source)
XLA Modules:
  0.0 91.1 jit_solution(15850760613756387396)
XLA Ops:
  0.6 88.2 %layer.1 = (bf16[64,2048]{1,0:T(8,128)(2,1)}, f32[2,512]{1,0:T(2,128)}) custom-call(bf16[64,2048]{1,0:T(8,128)(2,1)} %tokens.1, f32[1,2048]{1,0:T(1,128)} %bitcast.2, bf16[2048,128]{1,0:T(8,128)(2,1)} %w_query.1, bf16[2048,128]{1,0:T(8,128)(2,1)} %w_key.1, bf16[2048,128]{1,0:T(8,128)(2,1)} %w_value.1, bf16[2048,256]{1,0:T(8,128)(2,1)} %conv_in.1, ...), custom_call_target="tpu_custom_call" | custom-call | tf_op jit(solution)/shard_map/layer/pallas_call | solution.py:569
  88.8 0.0 copy-start
  88.9 1.7 %copy.16 = bf16[64,2048]{1,0:T(8,128)(2,1)} copy(bf16[64,2048]{1,0:T(8,128)(2,1)} %get-tuple-element.4) | data formatting | bytes 524288
  90.5 0.0 copy-done
  90.5 0.6 copy.17
Async XLA Ops:
  88.8 1.7 %copy-start = (f32[2,512]{1,0:T(2,128)S(1)}, f32[2,512]{1,0:T(2,128)}, u32[]{:S(2)}) copy-start(f32[2,512]{1,0:T(2,128)} %get-tuple-element.5) | copy-start | bytes 12292

commit v2 on v1

v2 whole, which is shorter than its diff:
```python
import functools

import jax
import jax.numpy as jnp
from jax import lax
from jax.experimental import pallas as pl
from jax.experimental.pallas import tpu as pltpu
from jax.sharding import PartitionSpec as P

MESH = pl.DeviceIdType.MESH
F32 = jnp.float32
BF16 = jnp.bfloat16
HEAD = 64
NX = 4
NY = 4
LOW = -1e30
LOG2E = 1.4426950408889634
VROWS = 80
AT_ONCE = 4


def kernel(
    tokens,
    norm_gain,
    w_query,
    w_key,
    w_value,
    conv_in,
    conv_gate,
    conv_taps,
    conv_gain,
    cum_gate,
    out_attn,
    out_conv,
    mixed,
    log_total,
    nt,
    wall,
    wo,
    wconv,
    qp,
    qb,
    ks,
    vs,
    kp,
    vp,
    cpad,
    mrow,
    acc,
    obuf,
    orecv,
    sbuf,
    srecv,
    gb,
    rim,
    cg,
    cv,
    sq,
    csq,
    xs,
    sb,
    rb,
    po,
    t2,
    r2r,
    r2l,
    sr,
    sl,
    frl,
    frr,
    at_out,
    at_in,
    lt_out,
    lt_in,
    wsem,
    gsend,
    grecv,
    wosend,
    worecv,
    ksend,
    krecv,
    vsend,
    vrecv,
    qsend,
    qrecv,
    qbsend,
    qbrecv,
    qrsend,
    qrrecv,
    msend,
    mrecv,
    osend,
    orecv_sem,
    csend,
    crecv,
    xsend,
    xrecv,
    asend,
    arecv,
    lsend,
    lrecv,
):
    s_me = lax.axis_index("sp")
    t_me = lax.axis_index("tp")
    nsp = lax.axis_size("sp")
    nz = nsp // NX
    z = s_me // NX
    x = s_me % NX
    y = t_me // 2
    c = t_me % 2
    rows = tokens.shape[0]
    half = rows // 2
    depth = tokens.shape[1]
    tok = rows * 8
    mid_tok = tok // 2
    zbar = nz - 1 - z

    def at_tp(t):
        return (s_me, t)

    def at_sp(s):
        return (s, t_me)

    def rcopy(src, dst, ssem, rsem, dev):
        return pltpu.make_async_remote_copy(
            src_ref=src,
            dst_ref=dst,
            send_sem=ssem,
            recv_sem=rsem,
            device_id=dev,
            device_id_type=MESH,
        )

    wcopies = []
    at = 0
    for i, w in enumerate((w_query, w_key, w_value, conv_in, conv_gate)):
        n = w.shape[1]
        wcopies.append(pltpu.make_async_copy(w, wall.at[:, pl.ds(at, n)], wsem.at[i]))
        at += n
    ocopies = [
        pltpu.make_async_copy(out_attn, wo.at[t_me], wsem.at[5]),
        pltpu.make_async_copy(out_conv, wconv, wsem.at[6]),
    ]
    for w in wcopies + ocopies:
        w.start()

    barrier = pltpu.get_barrier_semaphore()
    for d in range(1, 8):
        pl.semaphore_signal(
            barrier, inc=1, device_id=at_tp((t_me + d) % 8), device_id_type=MESH
        )
    for d in range(1, NX):
        pl.semaphore_signal(
            barrier, inc=1, device_id=at_sp(z * NX + (x + d) % NX), device_id_type=MESH
        )
    for d in (1, nz - 1):
        pl.semaphore_signal(
            barrier, inc=1, device_id=at_sp(((z + d) % nz) * NX + x), device_id_type=MESH
        )
    for d in (1, nsp - 1):
        pl.semaphore_signal(
            barrier, inc=1, device_id=at_sp((s_me + d) % nsp), device_id_type=MESH
        )

    for t in range(8):
        pl.semaphore_signal(
            barrier, inc=1, device_id=(zbar * NX + x, t), device_id_type=MESH
        )

    wide = tokens[...].astype(F32)
    factor = lax.rsqrt(jnp.mean(wide * wide, axis=1, keepdims=True) + 1e-06)
    nt[t_me] = (wide * factor * norm_gain[...]).astype(BF16)
    qp[:, 0, HEAD:, :] = jnp.ones((NX, HEAD, tok), BF16)
    qp[:, 1, :HEAD, :] = jnp.ones((NX, HEAD, tok), BF16)
    vp[:, HEAD:, :] = jnp.ones((2, VROWS - HEAD, tok), BF16)
    cpad[...] = jnp.zeros_like(cpad)
    mrow[...] = jnp.full_like(mrow, LOW)
    acc[...] = jnp.zeros_like(acc)

    pl.semaphore_wait(barrier, 7 + NX - 1 + 4 + 8)

    sib = y * 2 + (1 - c)
    tr = ((y + 1) % NY) * 2 + c
    tl = ((y + NY - 1) % NY) * 2 + c
    to = ((y + 2) % NY) * 2 + c
    lo, hi = pl.ds(0, half), pl.ds(half, half)

    def gather_over_tp(buf, ssem, rsem):
        n = buf.shape[1] // 2
        first, last = pl.ds(0, n), pl.ds(n, n)

        def gcopy(k, src, part, dev):
            ref = buf.at[src] if part is None else buf.at[src, part]
            return rcopy(ref, ref, ssem.at[k], rsem.at[k], at_tp(dev))

        return [
            gcopy(0, t_me, None, sib),
            gcopy(1, t_me, first, tr),
            gcopy(2, t_me, last, tr),
            gcopy(3, t_me, last, tl),
            gcopy(4, t_me, first, tl),
            gcopy(5, tl, None, sib),
            gcopy(6, tr, None, sib),
            gcopy(7, tl, first, tr),
            gcopy(8, tr, last, tl),
            gcopy(9, to, first, sib),
            gcopy(10, to, last, sib),
        ]

    g = gather_over_tp(nt, gsend, grecv)
    gw = gather_over_tp(wo, wosend, worecv)
    for k in (1, 3, 2, 4, 0):
        g[k].start()

    def sp_of(zz):
        return at_sp(zz * NX + x)

    def kcopy(zb, t, zt, part=None):
        ref = ks.at[zb] if part is None else ks.at[zb, part]
        return rcopy(ref, ref, ksend.at[t], krecv.at[t], sp_of(zt))

    def vcopy(zb, t, zt, part=None):
        ref = vs.at[zb] if part is None else vs.at[zb, :, part]
        return rcopy(ref, ref, vsend.at[t], vrecv.at[t], sp_of(zt))

    low_half, high_half = pl.ds(0, mid_tok), pl.ds(mid_tok, mid_tok)

    def qcopies(src, d, lanes, ssem, rsem):
        dev = at_sp(z * NX + (x + d) % NX)
        a = qp.at[src, 0, pl.ds(0, HEAD), lanes]
        b = qp.at[src, 1, pl.ds(HEAD, HEAD), lanes]
        return (
            rcopy(a, a, ssem.at[2 * d - 2], rsem.at[2 * d - 2], dev),
            rcopy(b, b, ssem.at[2 * d - 1], rsem.at[2 * d - 1], dev),
        )

    def qbcopies(src, lanes):
        dev = sp_of(zbar)
        return (
            rcopy(
                qb.at[pl.ds(0, HEAD), src],
                qp.at[x, 0, pl.ds(0, HEAD), lanes],
                qbsend.at[0],
                qbrecv.at[0],
                dev,
            ),
            rcopy(
                qb.at[pl.ds(HEAD, HEAD), src],
                qp.at[x, 1, pl.ds(HEAD, HEAD), lanes],
                qbsend.at[1],
                qbrecv.at[1],
                dev,
            ),
        )

    rcopy_rim = rcopy(
        gb.at[pl.ds(tok - 32, 32)], rim, msend.at[0], mrecv.at[0], at_sp((s_me + 1) % nsp)
    )
    for w in wcopies:
        w.wait()

    def project(i, carry):
        @pl.when(i == 0)
        def _():
            g[0].wait_recv()

        @pl.when(i == 1)
        def _():
            g[1].wait_recv()
            g[7].start()
            g[3].wait_recv()
            g[8].start()
            g[2].wait_recv()
            g[5].start()
            g[4].wait_recv()
            g[6].start()
            g[5].wait_recv()

        @pl.when(i == 2)
        def _():
            g[6].wait_recv()

        @pl.when(i == 3)
        def _():
            g[7].wait_recv()
            g[9].start()
            g[8].wait_recv()
            g[10].start()
            g[9].wait_recv()
            g[10].wait_recv()
            ocopies[0].wait()
            gw[1].start()
            gw[3].start()

        p = (y + 2 * NY - (2 * (i % 2) - 1) * ((i + 1) // 2)) % NY
        lhs = nt[pl.ds(2 * p, 2)].reshape(2 * rows, depth)
        res = jnp.dot(lhs, wall[...], preferred_element_type=F32)
        here = pl.ds(pl.multiple_of(p * 2 * rows, 2 * rows), 2 * rows)
        opened = res[:, 384:640]
        gating = res[:, 640:896]
        gate = (opened / (1.0 + jnp.exp(-gating))).astype(BF16)
        gb[here, :] = gate
        cg[pl.ds(pl.multiple_of(p * 2 * rows + 32, 32), 2 * rows), :] = gate.astype(F32)
        ks[z, here, :] = res[:, 128:256].astype(BF16)
        vs[z, :, here] = res[:, 256:384].T.astype(BF16)
        qt = (res[:, :128] * HEAD ** (-0.5)).T.astype(BF16)

        @pl.when(p < NY // 2)
        def _():
            qp[x, 0, :HEAD, here] = qt[:HEAD]
            qp[x, 1, HEAD:, here] = qt[HEAD:]

        qb[:, here] = qt

        @pl.when(p == NY - 1)
        def _():
            rcopy_rim.start()

        for t, zt in ((1, (z + 1) % nz), (2, (z + nz - 1) % nz)):
            kcopy(z, t, zt, here).start()
            vcopy(z, t, zt, here).start()

        @pl.when(p < NY // 2)
        def _():
            for d in (1, 3, 2):
                for q in qcopies(x, d, here, qsend, qrecv):
                    q.start()

        @pl.when(p >= NY // 2)
        def _():
            for q in qbcopies(here, here):
                q.start()

        return carry

    lax.fori_loop(0, NY, project, 0)

    rcopy_rim.wait_recv()
    first = jnp.where(s_me > 0, 1.0, 0.0).astype(F32)
    cg[0:32, :] = rim[...].astype(F32) * first

    def conv_rows(i, carry):
        r0 = pl.multiple_of(i * 64, 64)
        win = cg[pl.ds(r0, 96), :]
        total = jnp.zeros((64, win.shape[1]), F32)
        for b in range(8):
            turned = win if b == 0 else pltpu.roll(win, 96 - b, 0)
            for a in range(5):
                k = 8 * a + b - 2
                if 0 <= k < 31:
                    total = total + conv_taps[k : k + 1, :] * turned[8 * a : 8 * a + 64]
        cv[pl.ds(r0, 64), :] = total
        square = total * total
        sq[pl.ds(r0, 64), :] = square[:, :128] + square[:, 128:]
        return carry

    lax.fori_loop(0, tok // 64, conv_rows, 0)
    part = jnp.sum(sq[...].T, axis=0, keepdims=True)
    csq[t_me] = part
    ccopies = []
    for d in range(1, 8):
        cc = rcopy(
            csq.at[t_me], csq.at[t_me], csend.at[d], crecv.at[d], at_tp((t_me + d) % 8)
        )
        cc.start()
        ccopies.append(cc)
    for k in (2, 4, 0):
        gw[k].start()

    cref = cum_gate[:, pl.ds(pl.multiple_of(z * NX * tok, 128), 128)][:, :1]

    def prepare(zb):
        ck = cum_gate[:, pl.ds(pl.multiple_of((zb * NX + x) * tok, 128), tok)]
        bias = cref - ck
        high = bias.astype(BF16).astype(F32)
        left = bias - high
        mid = left.astype(BF16).astype(F32)
        low = left - mid
        rowid = lax.broadcasted_iota(jnp.int32, (8, tok), 0)
        for h, r0 in ((0, HEAD), (1, 0)):
            tile = jnp.where(
                rowid == 0,
                high[h : h + 1],
                jnp.where(
                    rowid == 1, mid[h : h + 1], jnp.where(rowid == 2, low[h : h + 1], 0.0)
                ),
            )
            cpad[r0 : r0 + 8, :] = tile
        extra = cpad[...].T
        kf = ks[zb].astype(F32)
        lane = lax.broadcasted_iota(jnp.int32, (tok, 2 * HEAD), 1)
        kp[0] = jnp.where(lane < HEAD, kf, extra).astype(BF16)
        kp[1] = jnp.where(lane < HEAD, extra, kf).astype(BF16)
        vp[0, :HEAD, :] = vs[zb, :HEAD, :]
        vp[1, :HEAD, :] = vs[zb, HEAD:, :]

    def chunks(js, g, masked):
        lanes = pl.ds(pl.multiple_of(g * mid_tok, mid_tok), mid_tok)
        units = [(j, h) for j in js for h in range(2)]
        old = [mrow[j, h, :, lanes] for j, h in units]
        held = [acc[j, h, :, lanes] for j, h in units]
        sc = [jnp.dot(kp[h], qp[j, h, :, lanes], preferred_element_type=F32) for j, h in units]
        if masked:
            kpos = lax.broadcasted_iota(jnp.int32, sc[0].shape, 0)
            qpos = lax.broadcasted_iota(jnp.int32, sc[0].shape, 1) + g * mid_tok
            sc = [jnp.where(kpos <= qpos, v, LOW) for v in sc]
        new = [jnp.maximum(o, jnp.max(v, axis=0, keepdims=True)) for o, v in zip(old, sc)]
        wts = [jnp.exp2((v - n) * LOG2E).astype(BF16) for n, v in zip(new, sc)]
        shrink = [jnp.exp2((o - n) * LOG2E) for o, n in zip(old, new)]
        out = [
            a * k + jnp.dot(vp[h], w, preferred_element_type=F32)
            for a, k, w, (_, h) in zip(held, shrink, wts, units)
        ]
        for n, o, (j, h) in zip(new, out, units):
            mrow[j, h, :, lanes] = n
            acc[j, h, :, lanes] = o

    def place(t):
        dr = 2 * (t % 2) - 1
        return dr, (z + nz - dr * ((t + 1) // 2)) % nz

    def ocopies_of(d, lanes, k):
        dev = at_sp(z * NX + (x + d) % NX)
        return (
            rcopy(
                obuf.at[d - 1, :, lanes],
                orecv.at[d - 1, :, lanes],
                osend.at[2 * k + 4 * (d - 1)],
                orecv_sem.at[2 * k + 4 * (d - 1)],
                dev,
            ),
            rcopy(
                sbuf.at[d - 1, :, lanes],
                srecv.at[d - 1, :, lanes],
                osend.at[2 * k + 4 * (d - 1) + 1],
                orecv_sem.at[2 * k + 4 * (d - 1) + 1],
                dev,
            ),
        )

    def final_at(zz, gg):
        zq = nz - 1 - zz if gg else zz
        order = [(zz - (2 * (t % 2) - 1) * ((t + 1) // 2)) % nz for t in range(nz)]
        return max(t for t in range(nz) if order[t] <= zq)

    def finish(t, g):
        done = False
        for zz in range(nz):
            for gg in range(2):
                done = done | ((z == zz) & (g == gg) & (t == final_at(zz, gg)))

        @pl.when(done)
        def _():
            lanes = pl.ds(pl.multiple_of(g * mid_tok, mid_tok), mid_tok)
            for d in (2, 1, 3):
                j = (x + d) % NX
                for h in range(2):
                    obuf[d - 1, h * HEAD : (h + 1) * HEAD, lanes] = acc[j, h, :HEAD, lanes].astype(
                        BF16
                    )
                    sbuf[d - 1, h : h + 1, lanes] = mrow[j, h, :, lanes]
                    sbuf[d - 1, 2 + h : 3 + h, lanes] = acc[j, h, HEAD : HEAD + 1, lanes]
                for cp in ocopies_of(d, lanes, g):
                    cp.start()

    def whole(g):
        def some(i, carry):
            chunks(tuple(i * AT_ONCE + k for k in range(AT_ONCE)), g, False)
            return carry

        lax.fori_loop(0, NX // AT_ONCE, some, 0)

    def diagonal(g):
        chunks((x,), g, True)

        def one(j, carry):
            chunks((j,), g, False)
            return carry

        lax.fori_loop(x + 1, NX, one, 0)

    def tile(t):
        _, zb = place(t)

        @pl.when((zb <= z) | (zb <= zbar))
        def _():
            prepare(zb)

            def group(i, carry):
                g = i + (z // (nz // 2)) * (1 - 2 * i)
                zq = z + g * (nz - 1 - 2 * z)

                @pl.when(zb < zq)
                def _():
                    whole(g)

                @pl.when(zb == zq)
                def _():
                    diagonal(g)

                @pl.when(zb <= zq)
                def _():
                    finish(t, g)

                return carry

            lax.fori_loop(0, 2, group, 0)

    def forward(t):
        dr, zb = place(t)
        zt = (z + nz + dr) % nz
        kcopy(zb, t, zt).wait_recv()
        if t <= 5:
            kcopy(zb, t + 2, zt).start()
        vcopy(zb, t, zt).wait_recv()
        if t <= 4 or t == 6:
            vcopy(zb, t + 2 - t // 6, zt).start()

    for d in range(1, NX):
        for q in qcopies(x, d, low_half, qsend, qrecv):
            q.wait_recv()
    prepare(z)
    diagonal(0)
    finish(0, 0)
    forward(1)
    forward(2)

    for q in qbcopies(high_half, high_half):
        q.wait_recv()
    for d in (1, 3, 2):
        for q in qcopies(x, d, high_half, qrsend, qrrecv):
            q.start()

    def project_out(which, emit):
        lhs = xs[which].reshape(NY * rows, xs.shape[3])

        def columns(n, carry):
            cols = pl.ds(pl.multiple_of(n * 512, 512), 512)
            res = jnp.dot(lhs, wconv[:, cols], preferred_element_type=F32)
            emit(cols, res)
            return carry

        lax.fori_loop(0, depth // 512, columns, 0)

    def emit_sib(cols, res):
        sb[:, :, cols] = res.astype(BF16).reshape(NY, rows, 512)

    def emit_own(cols, res):
        po[:, :, cols] = res.reshape(NY, rows, 512)

    ybits = [(y + k) % NY for k in range(NY)]

    def xcopy(k, src, dst, dev):
        return rcopy(src, dst, xsend.at[k], xrecv.at[k], at_tp(dev))

    bcopies = [xcopy(k, sb.at[ybits[k]], rb.at[ybits[k]], sib) for k in range(NY)]

    def conv_part():
        for cc in ccopies:
            cc.wait_recv()
        total = csq[0]
        for t in range(1, 8):
            total = total + csq[t]
        scale = lax.rsqrt(total / (8.0 * conv_gain.shape[1]) + 1e-06)
        sq[...] = jnp.broadcast_to(scale, (128, tok)).T
        for i in range(8):
            r = pl.ds(i * rows, rows)
            factor = sq[r, :]
            for b in range(2):
                lanes = pl.ds(b * 128, 128)
                v = cv[r, lanes] * factor * conv_gain[:, lanes]
                v = v / (1.0 + jnp.exp(-v))
                xs[i % 2, i // 2, :, lanes] = v.astype(BF16)
        ocopies[1].wait()

        project_out(1 - c, emit_sib)
        for k in (2, 1, 3, 0):
            bcopies[k].start()
        project_out(c, emit_own)

    far_r = xcopy(4, t2.at[lo], r2r, tr)
    far_l = xcopy(5, t2.at[hi], r2l, tl)
    near_r = xcopy(6, sr.at[hi], frl.at[hi], tr)
    near_l = xcopy(7, sl.at[lo], frr.at[lo], tl)
    both_r = xcopy(8, sr.at[lo], frl.at[lo], tr)
    both_l = xcopy(9, sl.at[hi], frr.at[hi], tl)

    def scatter_first():
        bcopies[2].wait_recv()
        t2[...] = (po[ybits[2]] + rb[ybits[2]].astype(F32)).astype(BF16)
        far_r.start()
        far_l.start()
        bcopies[1].wait_recv()
        sr[hi, :] = (po[ybits[1], hi] + rb[ybits[1], hi].astype(F32)).astype(BF16)
        near_r.start()
        bcopies[3].wait_recv()
        sl[lo, :] = (po[ybits[3], lo] + rb[ybits[3], lo].astype(F32)).astype(BF16)
        near_l.start()

    def scatter_second():
        far_r.wait_recv()
        sr[lo, :] = (
            po[ybits[1], lo] + rb[ybits[1], lo].astype(F32) + r2r[...].astype(F32)
        ).astype(BF16)
        both_r.start()
        far_l.wait_recv()
        sl[hi, :] = (
            po[ybits[3], hi] + rb[ybits[3], hi].astype(F32) + r2l[...].astype(F32)
        ).astype(BF16)
        both_l.start()
        bcopies[0].wait_recv()
        po[y] = po[y] + rb[y].astype(F32)

    def weights_on():
        for got, on in ((1, 7), (3, 8), (2, 5), (4, 6)):
            gw[got].wait_recv()
            gw[on].start()

    def weights_last():
        for got, on in ((7, 9), (8, 10)):
            gw[got].wait_recv()
            gw[on].start()

    conv_part()
    forward(3)
    forward(4)
    for d in range(1, NX):
        for q in qcopies(x, d, high_half, qrsend, qrrecv):
            q.wait_recv()

    @pl.when(z < zbar)
    def _():
        whole(1)

    def step(t, carry):
        tile(t)

        @pl.when(t == 1)
        def _():
            scatter_first()

        @pl.when(t == 3)
        def _():
            forward(5)
            forward(6)
            scatter_second()

        @pl.when(t == 4)
        def _():
            weights_on()

        @pl.when(t == 6)
        def _():
            forward(7)

        return carry

    lax.fori_loop(1, nz, step, 0)

    weights_last()

    for d in range(1, NX):
        for k, lanes in enumerate((low_half, high_half)):
            for cp in ocopies_of(d, lanes, k):
                cp.wait_recv()
    for h in range(2):
        best = mrow[x, h]
        for d in range(1, NX):
            best = jnp.maximum(best, srecv[d - 1, h : h + 1, :])
        share = jnp.exp2((mrow[x, h] - best) * LOG2E)
        summed = acc[x, h, HEAD : HEAD + 1, :] * share
        value = acc[x, h, :HEAD, :] * share
        for d in range(1, NX):
            share = jnp.exp2((srecv[d - 1, h : h + 1, :] - best) * LOG2E)
            summed = summed + srecv[d - 1, 2 + h : 3 + h, :] * share
            value = value + orecv[d - 1, h * HEAD : (h + 1) * HEAD, :].astype(F32) * share
        cpad[h * HEAD : (h + 1) * HEAD, :] = value / summed
        level = best + jnp.log(summed) - cref[h : h + 1]
        for zz, lanes, dst in ((z, low_half, log_total), (zbar, high_half, lt_out)):
            at = pl.multiple_of((zz * NX + x) * tok + lanes.start, 128)
            dst[h : h + 1, 0:mid_tok] = (
                level[:, lanes.start : lanes.start + mid_tok]
                + cum_gate[:, pl.ds(at, mid_tok)][h : h + 1]
            )
    at_out[...] = cpad[...].T.astype(BF16).reshape(8, rows, 2 * HEAD)

    mine = at_in.at[:, pl.ds(pl.multiple_of(t_me * 2 * HEAD, 2 * HEAD), 2 * HEAD)]
    lcopy = rcopy(lt_out, lt_in, lsend.at[0], lrecv.at[0], sp_of(zbar))

    def acopy(r):
        zz = z if r < 4 else zbar
        return rcopy(at_out.at[r], mine, asend.at[r], arecv.at[t_me], (zz * NX + x, r))

    for r in (4, 5, 6, 7):
        acopy(r).start()
    for r in (0, 1, 2, 3):

        @pl.when(t_me != r)
        def _(r=r):
            acopy(r).start()

    lcopy.start()

    @pl.when(t_me < 4)
    def _():
        mine[...] = at_out[t_me]

    for k in (0, 5, 6, 9, 10):
        gw[k].wait_recv()
    near_r.wait_recv()
    near_l.wait_recv()
    both_r.wait_recv()
    both_l.wait_recv()
    po[y] = po[y] + frl[...].astype(F32) + frr[...].astype(F32)
    for t in range(8):

        @pl.when((t_me >= 4) | (t_me != t))
        def _(t=t):
            rcopy(
                at_out.at[0],
                at_in.at[:, pl.ds(t * 2 * HEAD, 2 * HEAD)],
                asend.at[0],
                arecv.at[t],
                sp_of(zbar),
            ).wait_recv()

    lhs = at_in[...]

    def last(n, carry):
        cols = pl.ds(pl.multiple_of(n * 512, 512), 512)
        w = wo[:, :, cols].reshape(lhs.shape[1], 512)
        res = jnp.dot(lhs, w, preferred_element_type=F32)
        mixed[:, cols] = (po[y, :, cols] + res).astype(BF16)
        return carry

    lax.fori_loop(0, depth // 512, last, 0)
    lcopy.wait_recv()
    log_total[:, mid_tok:] = lt_in[0:2, :]

    for cp in g + gw:
        cp.wait_send()
    for t in range(1, 8):
        kcopy(z, t, (z + 1) % nz).wait_send()
        vcopy(z, t, (z + 1) % nz).wait_send()
    for d in range(1, NX):
        for q in qcopies(x, d, low_half, qsend, qrecv) + qcopies(x, d, high_half, qrsend, qrrecv):
            q.wait_send()
    for q in qbcopies(high_half, high_half):
        q.wait_send()
    rcopy_rim.wait_send()
    for d in range(1, NX):
        for k, lanes in enumerate((low_half, high_half)):
            for cp in ocopies_of(d, lanes, k):
                cp.wait_send()
    for cp in ccopies + bcopies:
        cp.wait_send()
    for cp in (far_r, far_l, near_r, near_l, both_r, both_l, lcopy):
        cp.wait_send()
    for r in (4, 5, 6, 7):
        acopy(r).wait_send()
    for r in (0, 1, 2, 3):

        @pl.when(t_me != r)
        def _(r=r):
            acopy(r).wait_send()


def per_device(*args):
    tokens = args[0]
    rows, depth = tokens.shape
    tok = rows * 8
    nz = lax.axis_size("sp") // NX
    att = args[2].shape[1]
    ch = args[5].shape[1]
    wide = 3 * att + 2 * ch
    ops = list(args)
    ops[1] = args[1][None]
    ops[8] = args[8][None]
    vmem = pl.BlockSpec(memory_space=pltpu.VMEM)
    hbm = pl.BlockSpec(memory_space=pltpu.HBM)
    specs = [vmem, vmem, hbm, hbm, hbm, hbm, hbm, vmem, vmem, vmem, hbm, hbm]
    dma = pltpu.SemaphoreType.DMA
    scratch = [
        pltpu.VMEM((8, rows, depth), BF16),
        pltpu.VMEM((depth, wide), BF16),
        pltpu.VMEM((8, att, depth), BF16),
        pltpu.VMEM((ch, depth), BF16),
        pltpu.VMEM((NX, 2, att, tok), BF16),
        pltpu.VMEM((att, tok), BF16),
        pltpu.VMEM((nz, tok, att), BF16),
        pltpu.VMEM((nz, att, tok), BF16),
        pltpu.VMEM((2, tok, att), BF16),
        pltpu.VMEM((2, VROWS, tok), BF16),
        pltpu.VMEM((att, tok), F32),
        pltpu.VMEM((NX, 2, 1, tok), F32),
        pltpu.VMEM((NX, 2, VROWS, tok), F32),
        pltpu.VMEM((NX - 1, att, tok), BF16),
        pltpu.VMEM((NX - 1, att, tok), BF16),
        pltpu.VMEM((NX - 1, 8, tok), F32),
        pltpu.VMEM((NX - 1, 8, tok), F32),
        pltpu.VMEM((tok, ch), BF16),
        pltpu.VMEM((32, ch), BF16),
        pltpu.VMEM((tok + 32, ch), F32),
        pltpu.VMEM((tok, ch), F32),
        pltpu.VMEM((tok, 128), F32),
        pltpu.VMEM((8, 1, tok), F32),
        pltpu.VMEM((2, NY, rows, ch), BF16),
        pltpu.VMEM((NY, rows, depth), BF16),
        pltpu.VMEM((NY, rows, depth), BF16),
        pltpu.VMEM((NY, rows, depth), F32),
        pltpu.VMEM((rows, depth), BF16),
        pltpu.VMEM((rows // 2, depth), BF16),
        pltpu.VMEM((rows // 2, depth), BF16),
        pltpu.VMEM((rows, depth), BF16),
        pltpu.VMEM((rows, depth), BF16),
        pltpu.VMEM((rows, depth), BF16),
        pltpu.VMEM((rows, depth), BF16),
        pltpu.VMEM((8, rows, att), BF16),
        pltpu.VMEM((rows, 8 * att), BF16),
        pltpu.VMEM((8, tok // 2), F32),
        pltpu.VMEM((8, tok // 2), F32),
    ] + [dma((n,)) for n in (7, 11, 11, 11, 11, 8, 8, 8, 8, 6, 6, 2, 2, 6, 6, 1, 1, 12, 12, 8, 8, 10, 10, 8, 8, 1, 1)]
    return pl.pallas_call(
        kernel,
        out_shape=(
            jax.ShapeDtypeStruct((rows, depth), BF16),
            jax.ShapeDtypeStruct((2, tok), F32),
        ),
        in_specs=specs,
        out_specs=(vmem, vmem),
        scratch_shapes=scratch,
        compiler_params=pltpu.CompilerParams(
            collective_id=0, has_side_effects=True, vmem_limit_bytes=58 * 1024 * 1024
        ),
        name="layer",
    )(*ops)


def solution(mesh):
    in_specs = (
        P(("sp", "tp"), None),
        P(),
        P(None, "tp"),
        P(None, "tp"),
        P(None, "tp"),
        P(None, "tp"),
        P(None, "tp"),
        P(None, "tp"),
        P("tp"),
        P("tp", None),
        P("tp", None),
        P("tp", None),
    )
    out_specs = (P(("sp", "tp"), None), P("tp", "sp"))
    return jax.shard_map(
        per_device, mesh=mesh, in_specs=in_specs, out_specs=out_specs, check_vma=False
    )
```

time: 91.2 us -> 72.6 us (0.80)
  the two profiles are of different devices: /device:TPU:228 before, /device:TPU:1 now
where the time goes in v2:
time: 72.6 us; the launch traced here: 71.9 us
  Pallas kernels  69 us (95%)
  local copies, waits for them, and re-layouts  2.27 us (3%)
    pallas_call x1, Pallas kernels, per_device(): pl.pallas_call(kernel, out_shape=(jax.ShapeDtypeStruct((rows, depth), BF1...  69 us
    unnamed x4, local copies, waits for them, and re-layouts  2.27 us

profile of v2, /device:TPU:1, one launch (start us, length us, event | category | flops | bytes accessed | tf_op | source)
XLA Modules:
  0.0 71.9 jit_solution(12747162315159510191)
XLA Ops:
  0.6 69.0 %layer.1 = (bf16[64,2048]{1,0:T(8,128)(2,1)}, f32[2,512]{1,0:T(2,128)}) custom-call(bf16[64,2048]{1,0:T(8,128)(2,1)} %tokens.1, f32[1,2048]{1,0:T(1,128)} %bitcast.2, bf16[2048,128]{1,0:T(8,128)(2,1)} %w_query.1, bf16[2048,128]{1,0:T(8,128)(2,1)} %w_key.1, bf16[2048,128]{1,0:T(8,128)(2,1)} %w_value.1, bf16[2048,256]{1,0:T(8,128)(2,1)} %conv_in.1, ...), custom_call_target="tpu_custom_call" | custom-call | tf_op jit(solution)/shard_map/layer/pallas_call | solution.py:823
  69.6 0.0 copy-start
  69.6 1.7 %copy.16 = bf16[64,2048]{1,0:T(8,128)(2,1)} copy(bf16[64,2048]{1,0:T(8,128)(2,1)} %get-tuple-element.4) | data formatting | bytes 524288
  71.3 0.0 copy-done
  71.3 0.6 copy.17
Async XLA Ops:
  69.6 1.7 %copy-start = (f32[2,512]{1,0:T(2,128)S(1)}, f32[2,512]{1,0:T(2,128)}, u32[]{:S(2)}) copy-start(f32[2,512]{1,0:T(2,128)} %get-tuple-element.5) | copy-start | bytes 12292

commit v3 on v2

--- a/solution.py
+++ b/solution.py
@@ -114,6 +114,8 @@
     tok = rows * 8
     mid_tok = tok // 2
     zbar = nz - 1 - z
+    hb = y // (NY // 2)
+    ha = 1 - hb
 
     def at_tp(t):
         return (s_me, t)
@@ -288,9 +290,6 @@
             g[10].start()
             g[9].wait_recv()
             g[10].wait_recv()
-            ocopies[0].wait()
-            gw[1].start()
-            gw[3].start()
 
         p = (y + 2 * NY - (2 * (i % 2) - 1) * ((i + 1) // 2)) % NY
         lhs = nt[pl.ds(2 * p, 2)].reshape(2 * rows, depth)
@@ -305,12 +304,14 @@
         vs[z, :, here] = res[:, 256:384].T.astype(BF16)
         qt = (res[:, :128] * HEAD ** (-0.5)).T.astype(BF16)
 
-        @pl.when(p < NY // 2)
-        def _():
-            qp[x, 0, :HEAD, here] = qt[:HEAD]
-            qp[x, 1, HEAD:, here] = qt[HEAD:]
-
-        qb[:, here] = qt
+        spot = pl.ds(pl.multiple_of((p % 2) * 2 * rows, 2 * rows), 2 * rows)
+        over = pl.ds(pl.multiple_of((p % 2) * 2 * rows + mid_tok, 2 * rows), 2 * rows)
+
+        @pl.when(p // 2 == hb)
+        def _():
+            qb[:, spot] = qt
+            for q in qbcopies(spot, over):
+                q.start()
 
         @pl.when(p == NY - 1)
         def _():
@@ -320,24 +321,17 @@
             kcopy(z, t, zt, here).start()
             vcopy(z, t, zt, here).start()
 
-        @pl.when(p < NY // 2)
-        def _():
+        @pl.when(p // 2 == ha)
+        def _():
+            qp[x, 0, :HEAD, spot] = qt[:HEAD]
+            qp[x, 1, HEAD:, spot] = qt[HEAD:]
             for d in (1, 3, 2):
-                for q in qcopies(x, d, here, qsend, qrecv):
+                for q in qcopies(x, d, spot, qsend, qrecv):
                     q.start()
 
-        @pl.when(p >= NY // 2)
-        def _():
-            for q in qbcopies(here, here):
-                q.start()
-
         return carry
 
     lax.fori_loop(0, NY, project, 0)
-
-    rcopy_rim.wait_recv()
-    first = jnp.where(s_me > 0, 1.0, 0.0).astype(F32)
-    cg[0:32, :] = rim[...].astype(F32) * first
 
     def conv_rows(i, carry):
         r0 = pl.multiple_of(i * 64, 64)
@@ -354,18 +348,7 @@
         sq[pl.ds(r0, 64), :] = square[:, :128] + square[:, 128:]
         return carry
 
-    lax.fori_loop(0, tok // 64, conv_rows, 0)
-    part = jnp.sum(sq[...].T, axis=0, keepdims=True)
-    csq[t_me] = part
-    ccopies = []
-    for d in range(1, 8):
-        cc = rcopy(
-            csq.at[t_me], csq.at[t_me], csend.at[d], crecv.at[d], at_tp((t_me + d) % 8)
-        )
-        cc.start()
-        ccopies.append(cc)
-    for k in (2, 4, 0):
-        gw[k].start()
+    lax.fori_loop(1, tok // 64, conv_rows, 0)
 
     cref = cum_gate[:, pl.ds(pl.multiple_of(z * NX * tok, 128), 128)][:, :1]
 
@@ -402,7 +385,8 @@
         sc = [jnp.dot(kp[h], qp[j, h, :, lanes], preferred_element_type=F32) for j, h in units]
         if masked:
             kpos = lax.broadcasted_iota(jnp.int32, sc[0].shape, 0)
-            qpos = lax.broadcasted_iota(jnp.int32, sc[0].shape, 1) + g * mid_tok
+            qpos = lax.broadcasted_iota(jnp.int32, sc[0].shape, 1)
+            qpos = qpos + (ha + g * (hb - ha)) * mid_tok
             sc = [jnp.where(kpos <= qpos, v, LOW) for v in sc]
         new = [jnp.maximum(o, jnp.max(v, axis=0, keepdims=True)) for o, v in zip(old, sc)]
         wts = [jnp.exp2((v - n) * LOG2E).astype(BF16) for n, v in zip(new, sc)]
@@ -506,26 +490,26 @@
 
             lax.fori_loop(0, 2, group, 0)
 
-    def forward(t):
+    def keys_on(t):
         dr, zb = place(t)
         zt = (z + nz + dr) % nz
         kcopy(zb, t, zt).wait_recv()
         if t <= 5:
             kcopy(zb, t + 2, zt).start()
+
+    def values_on(t):
+        dr, zb = place(t)
+        zt = (z + nz + dr) % nz
         vcopy(zb, t, zt).wait_recv()
         if t <= 4 or t == 6:
             vcopy(zb, t + 2 - t // 6, zt).start()
 
-    for d in range(1, NX):
-        for q in qcopies(x, d, low_half, qsend, qrecv):
-            q.wait_recv()
-    prepare(z)
-    diagonal(0)
-    finish(0, 0)
-    forward(1)
-    forward(2)
-
-    for q in qbcopies(high_half, high_half):
+    keys_on(1)
+    keys_on(2)
+    values_on(1)
+    values_on(2)
+
+    for q in qbcopies(low_half, high_half):
         q.wait_recv()
     for d in (1, 3, 2):
         for q in qcopies(x, d, high_half, qrsend, qrrecv):
@@ -621,9 +605,31 @@
             gw[got].wait_recv()
             gw[on].start()
 
-    conv_part()
-    forward(3)
-    forward(4)
+    rcopy_rim.wait_recv()
+    first = jnp.where(s_me > 0, 1.0, 0.0).astype(F32)
+    cg[0:32, :] = rim[...].astype(F32) * first
+    conv_rows(0, 0)
+    part = jnp.sum(sq[...].T, axis=0, keepdims=True)
+    csq[t_me] = part
+    ccopies = []
+    for d in range(1, 8):
+        cc = rcopy(
+            csq.at[t_me], csq.at[t_me], csend.at[d], crecv.at[d], at_tp((t_me + d) % 8)
+        )
+        cc.start()
+        ccopies.append(cc)
+    ocopies[0].wait()
+    for k in (1, 3, 2, 4, 0):
+        gw[k].start()
+
+    for d in range(1, NX):
+        for q in qcopies(x, d, low_half, qsend, qrecv):
+            q.wait_recv()
+    prepare(z)
+    diagonal(0)
+    finish(0, 0)
+    keys_on(3)
+    keys_on(4)
     for d in range(1, NX):
         for q in qcopies(x, d, high_half, qrsend, qrrecv):
             q.wait_recv()
@@ -632,32 +638,45 @@
     def _():
         whole(1)
 
-    def step(t, carry):
+    swap = ((z + 4) // nz) * ((2 * nz - 2 - z) // nz)
+
+    def step(i, carry):
+        early = (i // 2 % 2) * (1 - i // 4)
+        is_two, is_three = early * (1 - i % 2), early * (i % 2)
+        t = i + swap * (is_two - is_three)
         tile(t)
 
-        @pl.when(t == 1)
-        def _():
+        @pl.when(i == 1)
+        def _():
+            values_on(3)
+            values_on(4)
+            conv_part()
+            keys_on(5)
+            keys_on(6)
+
+        @pl.when(i == 2)
+        def _():
+            values_on(5)
+            values_on(6)
             scatter_first()
 
-        @pl.when(t == 3)
-        def _():
-            forward(5)
-            forward(6)
+        @pl.when(i == 4)
+        def _():
+            weights_on()
+
+        @pl.when(i == 5)
+        def _():
             scatter_second()
 
-        @pl.when(t == 4)
-        def _():
-            weights_on()
-
-        @pl.when(t == 6)
-        def _():
-            forward(7)
+        @pl.when(i == 6)
+        def _():
+            keys_on(7)
+            values_on(7)
 
         return carry
 
     lax.fori_loop(1, nz, step, 0)
 
-    weights_last()
 
     for d in range(1, NX):
         for k, lanes in enumerate((low_half, high_half)):
@@ -676,35 +695,29 @@
             value = value + orecv[d - 1, h * HEAD : (h + 1) * HEAD, :].astype(F32) * share
         cpad[h * HEAD : (h + 1) * HEAD, :] = value / summed
         level = best + jnp.log(summed) - cref[h : h + 1]
-        for zz, lanes, dst in ((z, low_half, log_total), (zbar, high_half, lt_out)):
-            at = pl.multiple_of((zz * NX + x) * tok + lanes.start, 128)
-            dst[h : h + 1, 0:mid_tok] = (
+        for zz, part, lanes, dst, at in (
+            (z, ha, low_half, log_total, pl.multiple_of(ha * mid_tok, mid_tok)),
+            (zbar, hb, high_half, lt_out, 0),
+        ):
+            here = pl.multiple_of((zz * NX + x) * tok + part * mid_tok, 128)
+            dst[h : h + 1, pl.ds(at, mid_tok)] = (
                 level[:, lanes.start : lanes.start + mid_tok]
-                + cum_gate[:, pl.ds(at, mid_tok)][h : h + 1]
+                + cum_gate[:, pl.ds(here, mid_tok)][h : h + 1]
             )
     at_out[...] = cpad[...].T.astype(BF16).reshape(8, rows, 2 * HEAD)
 
     mine = at_in.at[:, pl.ds(pl.multiple_of(t_me * 2 * HEAD, 2 * HEAD), 2 * HEAD)]
     lcopy = rcopy(lt_out, lt_in, lsend.at[0], lrecv.at[0], sp_of(zbar))
 
-    def acopy(r):
-        zz = z if r < 4 else zbar
-        return rcopy(at_out.at[r], mine, asend.at[r], arecv.at[t_me], (zz * NX + x, r))
-
-    for r in (4, 5, 6, 7):
-        acopy(r).start()
-    for r in (0, 1, 2, 3):
-
-        @pl.when(t_me != r)
-        def _(r=r):
-            acopy(r).start()
-
+    def acopy(k):
+        zz, owner = (z, 4 * ha + k) if k < 4 else (zbar, 4 * hb + k - 4)
+        return rcopy(at_out.at[k], mine, asend.at[k], arecv.at[t_me], (zz * NX + x, owner))
+
+    for k in (4, 5, 6, 7, 0, 1, 2, 3):
+        acopy(k).start()
     lcopy.start()
 
-    @pl.when(t_me < 4)
-    def _():
-        mine[...] = at_out[t_me]
-
+    weights_last()
     for k in (0, 5, 6, 9, 10):
         gw[k].wait_recv()
     near_r.wait_recv()
@@ -713,16 +726,13 @@
     both_l.wait_recv()
     po[y] = po[y] + frl[...].astype(F32) + frr[...].astype(F32)
     for t in range(8):
-
-        @pl.when((t_me >= 4) | (t_me != t))
-        def _(t=t):
-            rcopy(
-                at_out.at[0],
-                at_in.at[:, pl.ds(t * 2 * HEAD, 2 * HEAD)],
-                asend.at[0],
-                arecv.at[t],
-                sp_of(zbar),
-            ).wait_recv()
+        rcopy(
+            at_out.at[0],
+            at_in.at[:, pl.ds(t * 2 * HEAD, 2 * HEAD)],
+            asend.at[0],
+            arecv.at[t],
+            sp_of(zbar),
+        ).wait_recv()
 
     lhs = at_in[...]
 
@@ -735,7 +745,7 @@
 
     lax.fori_loop(0, depth // 512, last, 0)
     lcopy.wait_recv()
-    log_total[:, mid_tok:] = lt_in[0:2, :]
+    log_total[:, pl.ds(pl.multiple_of(hb * mid_tok, mid_tok), mid_tok)] = lt_in[0:2, :]
 
     for cp in g + gw:
         cp.wait_send()
@@ -745,7 +755,7 @@
     for d in range(1, NX):
         for q in qcopies(x, d, low_half, qsend, qrecv) + qcopies(x, d, high_half, qrsend, qrrecv):
             q.wait_send()
-    for q in qbcopies(high_half, high_half):
+    for q in qbcopies(low_half, high_half):
         q.wait_send()
     rcopy_rim.wait_send()
     for d in range(1, NX):
@@ -756,13 +766,8 @@
         cp.wait_send()
     for cp in (far_r, far_l, near_r, near_l, both_r, both_l, lcopy):
         cp.wait_send()
-    for r in (4, 5, 6, 7):
-        acopy(r).wait_send()
-    for r in (0, 1, 2, 3):
-
-        @pl.when(t_me != r)
-        def _(r=r):
-            acopy(r).wait_send()
+    for k in range(8):
+        acopy(k).wait_send()
 
 
 def per_device(*args):
@@ -786,7 +791,7 @@
         pltpu.VMEM((8, att, depth), BF16),
         pltpu.VMEM((ch, depth), BF16),
         pltpu.VMEM((NX, 2, att, tok), BF16),
-        pltpu.VMEM((att, tok), BF16),
+        pltpu.VMEM((att, tok // 2), BF16),
         pltpu.VMEM((nz, tok, att), BF16),
         pltpu.VMEM((nz, att, tok), BF16),
         pltpu.VMEM((2, tok, att), BF16),

time: 72.6 us -> 69.4 us (0.956)
  the two profiles are of different devices: /device:TPU:1 before, /device:TPU:11 now
where the time goes in v3:
time: 69.4 us; the launch traced here: 69.3 us
  Pallas kernels  66.4 us (96%)
  local copies, waits for them, and re-layouts  2.27 us (3%)
    pallas_call x1, Pallas kernels, per_device(): pl.pallas_call(kernel, out_shape=(jax.ShapeDtypeStruct((rows, depth), BF1...  66.4 us
    unnamed x4, local copies, waits for them, and re-layouts  2.27 us

profile of v3, /device:TPU:11, one launch (start us, length us, event | category | flops | bytes accessed | tf_op | source)
XLA Modules:
  0.0 69.3 jit_solution(11896360659465513531)
XLA Ops:
  0.6 66.4 %layer.1 = (bf16[64,2048]{1,0:T(8,128)(2,1)}, f32[2,512]{1,0:T(2,128)}) custom-call(bf16[64,2048]{1,0:T(8,128)(2,1)} %tokens.1, f32[1,2048]{1,0:T(1,128)} %bitcast.2, bf16[2048,128]{1,0:T(8,128)(2,1)} %w_query.1, bf16[2048,128]{1,0:T(8,128)(2,1)} %w_key.1, bf16[2048,128]{1,0:T(8,128)(2,1)} %w_value.1, bf16[2048,256]{1,0:T(8,128)(2,1)} %conv_in.1, ...), custom_call_target="tpu_custom_call" | custom-call | tf_op jit(solution)/shard_map/layer/pallas_call | solution.py:828
  67.0 0.0 copy-start
  67.0 1.7 %copy.16 = bf16[64,2048]{1,0:T(8,128)(2,1)} copy(bf16[64,2048]{1,0:T(8,128)(2,1)} %get-tuple-element.4) | data formatting | bytes 524288
  68.7 0.0 copy-done
  68.7 0.6 copy.17
Async XLA Ops:
  67.0 1.7 %copy-start = (f32[2,512]{1,0:T(2,128)S(1)}, f32[2,512]{1,0:T(2,128)}, u32[]{:S(2)}) copy-start(f32[2,512]{1,0:T(2,128)} %get-tuple-element.5) | copy-start | bytes 12292

commit v4 on v3

--- a/solution.py
+++ b/solution.py
@@ -27,13 +27,18 @@
     w_value,
     conv_in,
     conv_gate,
+    taps_hbm,
+    gain_hbm,
+    cum_hbm,
+    out_attn,
+    out_conv,
+    mixed_hbm,
+    log_hbm,
+    mixed,
+    log_total,
     conv_taps,
     conv_gain,
     cum_gate,
-    out_attn,
-    out_conv,
-    mixed,
-    log_total,
     nt,
     wall,
     wo,
@@ -143,7 +148,13 @@
         pltpu.make_async_copy(out_attn, wo.at[t_me], wsem.at[5]),
         pltpu.make_async_copy(out_conv, wconv, wsem.at[6]),
     ]
-    for w in wcopies + ocopies:
+    scopies = [
+        pltpu.make_async_copy(src, dst, wsem.at[7 + i])
+        for i, (src, dst) in enumerate(
+            ((taps_hbm, conv_taps), (gain_hbm, conv_gain), (cum_hbm, cum_gate))
+        )
+    ]
+    for w in wcopies + ocopies + scopies:
         w.start()
 
     barrier = pltpu.get_barrier_semaphore()
@@ -224,6 +235,25 @@
     def vcopy(zb, t, zt, part=None):
         ref = vs.at[zb] if part is None else vs.at[zb, :, part]
         return rcopy(ref, ref, vsend.at[t], vrecv.at[t], sp_of(zt))
+
+    def delivered(kind, t):
+        up, s = t % 2 == 1, (t + 1) // 2
+        if t == nz - 1:
+            up = kind == "k"
+        last = nz // 2 if up == (kind == "k") else nz // 2 - 1
+        rows_at = []
+        for zz in range(nz):
+            zb = (zz - s if up else zz + s) % nz
+            behind = [(zz + k if up else zz - k) % nz for k in range(last - s + 1)]
+            if any(zb <= max(r, nz - 1 - r) for r in behind):
+                rows_at.append(zz)
+        return rows_at
+
+    def among(kind, t, zz):
+        found = False
+        for r in delivered(kind, t):
+            found = found | (zz == r)
+        return found
 
     low_half, high_half = pl.ds(0, mid_tok), pl.ds(mid_tok, mid_tok)
 
@@ -258,7 +288,7 @@
     rcopy_rim = rcopy(
         gb.at[pl.ds(tok - 32, 32)], rim, msend.at[0], mrecv.at[0], at_sp((s_me + 1) % nsp)
     )
-    for w in wcopies:
+    for w in wcopies + scopies:
         w.wait()
 
     def project(i, carry):
@@ -318,8 +348,14 @@
             rcopy_rim.start()
 
         for t, zt in ((1, (z + 1) % nz), (2, (z + nz - 1) % nz)):
-            kcopy(z, t, zt, here).start()
-            vcopy(z, t, zt, here).start()
+
+            @pl.when(among("k", t, zt))
+            def _(t=t, zt=zt):
+                kcopy(z, t, zt, here).start()
+
+            @pl.when(among("v", t, zt))
+            def _(t=t, zt=zt):
+                vcopy(z, t, zt, here).start()
 
         @pl.when(p // 2 == ha)
         def _():
@@ -386,8 +422,8 @@
         if masked:
             kpos = lax.broadcasted_iota(jnp.int32, sc[0].shape, 0)
             qpos = lax.broadcasted_iota(jnp.int32, sc[0].shape, 1)
-            qpos = qpos + (ha + g * (hb - ha)) * mid_tok
-            sc = [jnp.where(kpos <= qpos, v, LOW) for v in sc]
+            ahead = kpos - qpos - (ha + g * (hb - ha)) * mid_tok
+            sc = [jnp.where(ahead <= (j - x) * tok, v, LOW) for v, (j, _) in zip(sc, units)]
         new = [jnp.maximum(o, jnp.max(v, axis=0, keepdims=True)) for o, v in zip(old, sc)]
         wts = [jnp.exp2((v - n) * LOG2E).astype(BF16) for n, v in zip(new, sc)]
         shrink = [jnp.exp2((o - n) * LOG2E) for o, n in zip(old, new)]
@@ -455,13 +491,7 @@
         lax.fori_loop(0, NX // AT_ONCE, some, 0)
 
     def diagonal(g):
-        chunks((x,), g, True)
-
-        def one(j, carry):
-            chunks((j,), g, False)
-            return carry
-
-        lax.fori_loop(x + 1, NX, one, 0)
+        chunks(tuple(range(NX)), g, True)
 
     def tile(t):
         _, zb = place(t)
@@ -493,16 +523,31 @@
     def keys_on(t):
         dr, zb = place(t)
         zt = (z + nz + dr) % nz
-        kcopy(zb, t, zt).wait_recv()
+
+        @pl.when(among("k", t, z))
+        def _():
+            kcopy(zb, t, zt).wait_recv()
+
         if t <= 5:
-            kcopy(zb, t + 2, zt).start()
+
+            @pl.when(among("k", t + 2, zt))
+            def _():
+                kcopy(zb, t + 2, zt).start()
 
     def values_on(t):
         dr, zb = place(t)
         zt = (z + nz + dr) % nz
-        vcopy(zb, t, zt).wait_recv()
+
+        @pl.when(among("v", t, z))
+        def _():
+            vcopy(zb, t, zt).wait_recv()
+
         if t <= 4 or t == 6:
-            vcopy(zb, t + 2 - t // 6, zt).start()
+            on = t + 2 - t // 6
+
+            @pl.when(among("v", on, zt))
+            def _():
+                vcopy(zb, on, zt).start()
 
     keys_on(1)
     keys_on(2)
@@ -664,14 +709,11 @@
         def _():
             weights_on()
 
-        @pl.when(i == 5)
-        def _():
-            scatter_second()
-
         @pl.when(i == 6)
         def _():
             keys_on(7)
             values_on(7)
+            scatter_second()
 
         return carry
 
@@ -736,22 +778,37 @@
 
     lhs = at_in[...]
 
+    lcopy.wait_recv()
+    log_total[:, pl.ds(pl.multiple_of(hb * mid_tok, mid_tok), mid_tok)] = lt_in[0:2, :]
+    log_put = pltpu.make_async_copy(log_total, log_hbm, wsem.at[10])
+    log_put.start()
+
+    def put(cols):
+        return pltpu.make_async_copy(mixed.at[:, cols], mixed_hbm.at[:, cols], wsem.at[11])
+
     def last(n, carry):
         cols = pl.ds(pl.multiple_of(n * 512, 512), 512)
         w = wo[:, :, cols].reshape(lhs.shape[1], 512)
         res = jnp.dot(lhs, w, preferred_element_type=F32)
         mixed[:, cols] = (po[y, :, cols] + res).astype(BF16)
+        put(cols).start()
         return carry
 
     lax.fori_loop(0, depth // 512, last, 0)
-    lcopy.wait_recv()
-    log_total[:, pl.ds(pl.multiple_of(hb * mid_tok, mid_tok), mid_tok)] = lt_in[0:2, :]
 
     for cp in g + gw:
         cp.wait_send()
     for t in range(1, 8):
-        kcopy(z, t, (z + 1) % nz).wait_send()
-        vcopy(z, t, (z + 1) % nz).wait_send()
+        above, below = (z + 1) % nz, (z + nz - 1) % nz
+
+        @pl.when(among("k", t, above if t % 2 else below))
+        def _(t=t, above=above):
+            kcopy(z, t, above).wait_send()
+
+        @pl.when(among("v", t, above if t % 2 and t < nz - 1 else below))
+        def _(t=t, above=above):
+            vcopy(z, t, above).wait_send()
+
     for d in range(1, NX):
         for q in qcopies(x, d, low_half, qsend, qrecv) + qcopies(x, d, high_half, qrsend, qrrecv):
             q.wait_send()
@@ -768,6 +825,8 @@
         cp.wait_send()
     for k in range(8):
         acopy(k).wait_send()
+    log_put.wait()
+    put(pl.ds(0, depth)).wait()
 
 
 def per_device(*args):
@@ -783,9 +842,14 @@
     ops[8] = args[8][None]
     vmem = pl.BlockSpec(memory_space=pltpu.VMEM)
     hbm = pl.BlockSpec(memory_space=pltpu.HBM)
-    specs = [vmem, vmem, hbm, hbm, hbm, hbm, hbm, vmem, vmem, vmem, hbm, hbm]
+    specs = [vmem, vmem] + [hbm] * 10
     dma = pltpu.SemaphoreType.DMA
     scratch = [
+        pltpu.VMEM((rows, depth), BF16),
+        pltpu.VMEM((2, tok), F32),
+        pltpu.VMEM(args[7].shape, F32),
+        pltpu.VMEM((1, ch), F32),
+        pltpu.VMEM(args[9].shape, F32),
         pltpu.VMEM((8, rows, depth), BF16),
         pltpu.VMEM((depth, wide), BF16),
         pltpu.VMEM((8, att, depth), BF16),
@@ -824,7 +888,7 @@
         pltpu.VMEM((rows, 8 * att), BF16),
         pltpu.VMEM((8, tok // 2), F32),
         pltpu.VMEM((8, tok // 2), F32),
-    ] + [dma((n,)) for n in (7, 11, 11, 11, 11, 8, 8, 8, 8, 6, 6, 2, 2, 6, 6, 1, 1, 12, 12, 8, 8, 10, 10, 8, 8, 1, 1)]
+    ] + [dma((n,)) for n in (12, 11, 11, 11, 11, 8, 8, 8, 8, 6, 6, 2, 2, 6, 6, 1, 1, 12, 12, 8, 8, 10, 10, 8, 8, 1, 1)]
     return pl.pallas_call(
         kernel,
         out_shape=(
@@ -832,7 +896,7 @@
             jax.ShapeDtypeStruct((2, tok), F32),
         ),
         in_specs=specs,
-        out_specs=(vmem, vmem),
+        out_specs=(hbm, hbm),
         scratch_shapes=scratch,
         compiler_params=pltpu.CompilerParams(
             collective_id=0, has_side_effects=True, vmem_limit_bytes=58 * 1024 * 1024

time: 69.4 us -> 69.4 us (level)
  the two profiles are of different devices: /device:TPU:11 before, /device:TPU:1 now
where the time goes in v4:
time: 69.4 us; the launch traced here: 69.3 us
  Pallas kernels  66.3 us (96%)
  local copies, waits for them, and re-layouts  2.27 us (3%)
    pallas_call x1, Pallas kernels, per_device(): pl.pallas_call(kernel, out_shape=(jax.ShapeDtypeStruct((rows, depth), BF1...  66.3 us
    unnamed x4, local copies, waits for them, and re-layouts  2.27 us

profile of v4, /device:TPU:1, one launch (start us, length us, event | category | flops | bytes accessed | tf_op | source)
XLA Modules:
  0.0 69.3 jit_solution(2645300517374964800)
XLA Ops:
  0.6 66.3 %layer.1 = (bf16[64,2048]{1,0:T(8,128)(2,1)}, f32[2,512]{1,0:T(2,128)}) custom-call(bf16[64,2048]{1,0:T(8,128)(2,1)} %tokens.1, f32[1,2048]{1,0:T(1,128)} %bitcast.2, bf16[2048,128]{1,0:T(8,128)(2,1)} %w_query.1, bf16[2048,128]{1,0:T(8,128)(2,1)} %w_key.1, bf16[2048,128]{1,0:T(8,128)(2,1)} %w_value.1, bf16[2048,256]{1,0:T(8,128)(2,1)} %conv_in.1, ...), custom_call_target="tpu_custom_call" | custom-call | tf_op jit(solution)/shard_map/layer/pallas_call | solution.py:892
  67.0 0.0 copy-start
  67.0 1.7 %copy.16 = bf16[64,2048]{1,0:T(8,128)(2,1)} copy(bf16[64,2048]{1,0:T(8,128)(2,1)} %get-tuple-element.4) | data formatting | bytes 524288
  68.7 0.0 copy-done
  68.7 0.6 copy.17
Async XLA Ops:
  67.0 1.7 %copy-start = (f32[2,512]{1,0:T(2,128)S(1)}, f32[2,512]{1,0:T(2,128)}, u32[]{:S(2)}) copy-start(f32[2,512]{1,0:T(2,128)} %get-tuple-element.5) | copy-start | bytes 12292

commit v5 on v4

--- a/solution.py
+++ b/solution.py
@@ -32,8 +32,6 @@
     cum_hbm,
     out_attn,
     out_conv,
-    mixed_hbm,
-    log_hbm,
     mixed,
     log_total,
     conv_taps,
@@ -228,13 +226,26 @@
     def sp_of(zz):
         return at_sp(zz * NX + x)
 
-    def kcopy(zb, t, zt, part=None):
+    def landed(t, piece):
+        return t if piece is None else 4 + 4 * t + piece
+
+    def kcopy(zb, t, zt, part=None, piece=None):
         ref = ks.at[zb] if part is None else ks.at[zb, part]
-        return rcopy(ref, ref, ksend.at[t], krecv.at[t], sp_of(zt))
-
-    def vcopy(zb, t, zt, part=None):
+        return rcopy(ref, ref, ksend.at[t], krecv.at[landed(t, piece)], sp_of(zt))
+
+    def vcopy(zb, t, zt, part=None, piece=None):
         ref = vs.at[zb] if part is None else vs.at[zb, :, part]
-        return rcopy(ref, ref, vsend.at[t], vrecv.at[t], sp_of(zt))
+        return rcopy(ref, ref, vsend.at[t], vrecv.at[landed(t, piece)], sp_of(zt))
+
+    def pair(i):
+        return (y + 2 * NY - (2 * (i % 2) - 1) * ((i + 1) // 2)) % NY
+
+    def pair_rows(i):
+        return pl.ds(pl.multiple_of(pair(i) * 2 * rows, 2 * rows), 2 * rows)
+
+    def place(t):
+        dr = 2 * (t % 2) - 1
+        return dr, (z + nz - dr * ((t + 1) // 2)) % nz
 
     def delivered(kind, t):
         up, s = t % 2 == 1, (t + 1) // 2
@@ -254,6 +265,21 @@
         for r in delivered(kind, t):
             found = found | (zz == r)
         return found
+
+    def piece_on(kind, piece):
+        copy = kcopy if kind == "k" else vcopy
+        part = pair_rows(piece)
+        for t in (1, 2):
+            dr, zb = place(t)
+            zt = (z + nz + dr) % nz
+
+            @pl.when(among(kind, t, z))
+            def _(t=t, zb=zb, zt=zt):
+                copy(zb, t, zt, part, piece).wait_recv()
+
+            @pl.when(among(kind, t + 2, zt))
+            def _(t=t, zb=zb, zt=zt):
+                copy(zb, t + 2, zt, part).start()
 
     low_half, high_half = pl.ds(0, mid_tok), pl.ds(mid_tok, mid_tok)
 
@@ -306,6 +332,8 @@
             g[5].start()
             g[4].wait_recv()
             g[6].start()
+            piece_on("k", 0)
+            piece_on("v", 0)
             g[5].wait_recv()
 
         @pl.when(i == 2)
@@ -321,10 +349,10 @@
             g[9].wait_recv()
             g[10].wait_recv()
 
-        p = (y + 2 * NY - (2 * (i % 2) - 1) * ((i + 1) // 2)) % NY
+        p = pair(i)
         lhs = nt[pl.ds(2 * p, 2)].reshape(2 * rows, depth)
         res = jnp.dot(lhs, wall[...], preferred_element_type=F32)
-        here = pl.ds(pl.multiple_of(p * 2 * rows, 2 * rows), 2 * rows)
+        here = pair_rows(i)
         opened = res[:, 384:640]
         gating = res[:, 640:896]
         gate = (opened / (1.0 + jnp.exp(-gating))).astype(BF16)
@@ -351,11 +379,11 @@
 
             @pl.when(among("k", t, zt))
             def _(t=t, zt=zt):
-                kcopy(z, t, zt, here).start()
+                kcopy(z, t, zt, here, i).start()
 
             @pl.when(among("v", t, zt))
             def _(t=t, zt=zt):
-                vcopy(z, t, zt, here).start()
+                vcopy(z, t, zt, here, i).start()
 
         @pl.when(p // 2 == ha)
         def _():
@@ -368,6 +396,9 @@
         return carry
 
     lax.fori_loop(0, NY, project, 0)
+
+    piece_on("k", 1)
+    piece_on("v", 1)
 
     def conv_rows(i, carry):
         r0 = pl.multiple_of(i * 64, 64)
@@ -435,10 +466,6 @@
             mrow[j, h, :, lanes] = n
             acc[j, h, :, lanes] = o
 
-    def place(t):
-        dr = 2 * (t % 2) - 1
-        return dr, (z + nz - dr * ((t + 1) // 2)) % nz
-
     def ocopies_of(d, lanes, k):
         dev = at_sp(z * NX + (x + d) % NX)
         return (
@@ -549,16 +576,27 @@
             def _():
                 vcopy(zb, on, zt).start()
 
-    keys_on(1)
-    keys_on(2)
-    values_on(1)
-    values_on(2)
-
-    for q in qbcopies(low_half, high_half):
-        q.wait_recv()
-    for d in (1, 3, 2):
-        for q in qcopies(x, d, high_half, qrsend, qrrecv):
-            q.start()
+    near = (z % 4) * (3 - z % 4) == 0
+    late = (z == 5) | (z == 6)
+
+    def relay():
+        for q in qbcopies(low_half, high_half):
+            q.wait_recv()
+        for d in (1, 3, 2):
+            for q in qcopies(x, d, high_half, qrsend, qrrecv):
+                q.start()
+
+    def relayed():
+        for d in range(1, NX):
+            for q in qcopies(x, d, high_half, qrsend, qrrecv):
+                q.wait_recv()
+
+    @pl.when(near)
+    def _():
+        relay()
+
+    for kind, piece in (("k", 2), ("v", 2), ("k", 3), ("v", 3)):
+        piece_on(kind, piece)
 
     def project_out(which, emit):
         lhs = xs[which].reshape(NY * rows, xs.shape[3])
@@ -667,21 +705,36 @@
     for k in (1, 3, 2, 4, 0):
         gw[k].start()
 
+    @pl.when(jnp.logical_not(near | late))
+    def _():
+        relay()
+
     for d in range(1, NX):
         for q in qcopies(x, d, low_half, qsend, qrecv):
             q.wait_recv()
     prepare(z)
     diagonal(0)
     finish(0, 0)
+    @pl.when(late)
+    def _():
+        relay()
+
     keys_on(3)
     keys_on(4)
-    for d in range(1, NX):
-        for q in qcopies(x, d, high_half, qrsend, qrrecv):
-            q.wait_recv()
+    @pl.when(jnp.logical_not(late))
+    def _():
+        relayed()
 
     @pl.when(z < zbar)
     def _():
         whole(1)
+
+    mid_row = nz // 2
+
+    @pl.when(z <= mid_row)
+    def _():
+        values_on(3)
+        values_on(4)
 
     swap = ((z + 4) // nz) * ((2 * nz - 2 - z) // nz)
 
@@ -693,17 +746,32 @@
 
         @pl.when(i == 1)
         def _():
-            values_on(3)
-            values_on(4)
+            @pl.when(z > mid_row)
+            def _():
+                values_on(3)
+                values_on(4)
+
+            @pl.when(z <= mid_row)
+            def _():
+                keys_on(5)
+                keys_on(6)
+
             conv_part()
-            keys_on(5)
-            keys_on(6)
+            @pl.when(z > mid_row)
+            def _():
+                keys_on(5)
+                keys_on(6)
+
 
         @pl.when(i == 2)
         def _():
             values_on(5)
             values_on(6)
             scatter_first()
+
+        @pl.when((i == 3) & late)
+        def _():
+            relayed()
 
         @pl.when(i == 4)
         def _():
@@ -780,18 +848,12 @@
 
     lcopy.wait_recv()
     log_total[:, pl.ds(pl.multiple_of(hb * mid_tok, mid_tok), mid_tok)] = lt_in[0:2, :]
-    log_put = pltpu.make_async_copy(log_total, log_hbm, wsem.at[10])
-    log_put.start()
-
-    def put(cols):
-        return pltpu.make_async_copy(mixed.at[:, cols], mixed_hbm.at[:, cols], wsem.at[11])
 
     def last(n, carry):
         cols = pl.ds(pl.multiple_of(n * 512, 512), 512)
         w = wo[:, :, cols].reshape(lhs.shape[1], 512)
         res = jnp.dot(lhs, w, preferred_element_type=F32)
         mixed[:, cols] = (po[y, :, cols] + res).astype(BF16)
-        put(cols).start()
         return carry
 
     lax.fori_loop(0, depth // 512, last, 0)
@@ -825,8 +887,6 @@
         cp.wait_send()
     for k in range(8):
         acopy(k).wait_send()
-    log_put.wait()
-    put(pl.ds(0, depth)).wait()
 
 
 def per_device(*args):
@@ -845,8 +905,6 @@
     specs = [vmem, vmem] + [hbm] * 10
     dma = pltpu.SemaphoreType.DMA
     scratch = [
-        pltpu.VMEM((rows, depth), BF16),
-        pltpu.VMEM((2, tok), F32),
         pltpu.VMEM(args[7].shape, F32),
         pltpu.VMEM((1, ch), F32),
         pltpu.VMEM(args[9].shape, F32),
@@ -888,15 +946,15 @@
         pltpu.VMEM((rows, 8 * att), BF16),
         pltpu.VMEM((8, tok // 2), F32),
         pltpu.VMEM((8, tok // 2), F32),
-    ] + [dma((n,)) for n in (12, 11, 11, 11, 11, 8, 8, 8, 8, 6, 6, 2, 2, 6, 6, 1, 1, 12, 12, 8, 8, 10, 10, 8, 8, 1, 1)]
+    ] + [dma((n,)) for n in (10, 11, 11, 11, 11, 8, 16, 8, 16, 6, 6, 2, 2, 6, 6, 1, 1, 12, 12, 8, 8, 10, 10, 8, 8, 1, 1)]
     return pl.pallas_call(
         kernel,
         out_shape=(
-            jax.ShapeDtypeStruct((rows, depth), BF16),
-            jax.ShapeDtypeStruct((2, tok), F32),
+            pltpu.VMEM((rows, depth), BF16),
+            pltpu.VMEM((2, tok), F32),
         ),
         in_specs=specs,
-        out_specs=(hbm, hbm),
+        out_specs=(vmem, vmem),
         scratch_shapes=scratch,
         compiler_params=pltpu.CompilerParams(
             collective_id=0, has_side_effects=True, vmem_limit_bytes=58 * 1024 * 1024

time: 69.4 us -> 66.8 us (0.963)
  Pallas kernels: 66.3 us -> 64.8 us
  local copies, waits for them, and re-layouts: 2.27 us -> 1.3 us
    pallas_call x1, Pallas kernels: 66.3 us -> 64.8 us  [per_device(): pl.pallas_call(kernel, out_shape=(pltpu.VMEM((rows, depth), BF16), pltpu....]
    unnamed x4 -> x2, local copies, waits for them, and re-layouts: 2.27 us -> 1.3 us
where the time goes in v5:
time: 66.8 us; the launch traced here: 66.7 us
  Pallas kernels  64.8 us (97%)
  local copies, waits for them, and re-layouts  1.3 us (2%)
    pallas_call x1, Pallas kernels, per_device(): pl.pallas_call(kernel, out_shape=(pltpu.VMEM((rows, depth), BF16), pltpu....  64.8 us

profile of v5, /device:TPU:1, one launch (start us, length us, event | category | flops | bytes accessed | tf_op | source)
XLA Modules:
  0.0 66.7 jit_solution(15110336144961382616)
XLA Ops:
  0.6 64.8 %layer.1 = (bf16[64,2048]{1,0:T(8,128)(2,1)S(1)}, f32[2,512]{1,0:T(2,128)S(1)}) custom-call(bf16[64,2048]{1,0:T(8,128)(2,1)} %tokens.1, f32[1,2048]{1,0:T(1,128)} %bitcast.2, bf16[2048,128]{1,0:T(8,128)(2,1)} %w_query.1, bf16[2048,128]{1,0:T(8,128)(2,1)} %w_key.1, bf16[2048,128]{1,0:T(8,128)(2,1)} %w_value.1, bf16[2048,256]{1,0:T(8,128)(2,1)} %conv_in.1, ...), custom_call_target="tpu_custom_call" | custom-call | tf_op jit(solution)/shard_map/layer/pallas_call | solution.py:950
  65.4 0.7 %copy.16 = bf16[64,2048]{1,0:T(8,128)(2,1)} copy(bf16[64,2048]{1,0:T(8,128)(2,1)S(1)} %get-tuple-element.2) | data formatting | bytes 524288
  66.1 0.6 copy.17

commit v6 on v5

--- a/solution.py
+++ b/solution.py
@@ -138,7 +138,7 @@
 
     wcopies = []
     at = 0
-    for i, w in enumerate((w_query, w_key, w_value, conv_in, conv_gate)):
+    for i, w in enumerate((w_key, w_value, w_query, conv_in, conv_gate)):
         n = w.shape[1]
         wcopies.append(pltpu.make_async_copy(w, wall.at[:, pl.ds(at, n)], wsem.at[i]))
         at += n
@@ -351,15 +351,26 @@
 
         p = pair(i)
         lhs = nt[pl.ds(2 * p, 2)].reshape(2 * rows, depth)
-        res = jnp.dot(lhs, wall[...], preferred_element_type=F32)
         here = pair_rows(i)
-        opened = res[:, 384:640]
-        gating = res[:, 640:896]
+        kv = jnp.dot(lhs, wall[:, :256], preferred_element_type=F32)
+        ks[z, here, :] = kv[:, :128].astype(BF16)
+        vs[z, :, here] = kv[:, 128:].T.astype(BF16)
+        for t, zt in ((1, (z + 1) % nz), (2, (z + nz - 1) % nz)):
+
+            @pl.when(among("k", t, zt))
+            def _(t=t, zt=zt):
+                kcopy(z, t, zt, here, i).start()
+
+            @pl.when(among("v", t, zt))
+            def _(t=t, zt=zt):
+                vcopy(z, t, zt, here, i).start()
+
+        res = jnp.dot(lhs, wall[:, 256:], preferred_element_type=F32)
+        opened = res[:, 128:384]
+        gating = res[:, 384:640]
         gate = (opened / (1.0 + jnp.exp(-gating))).astype(BF16)
         gb[here, :] = gate
-        cg[pl.ds(pl.multiple_of(p * 2 * rows + 32, 32), 2 * rows), :] = gate.astype(F32)
-        ks[z, here, :] = res[:, 128:256].astype(BF16)
-        vs[z, :, here] = res[:, 256:384].T.astype(BF16)
+        cg[pl.ds(pl.multiple_of(pair(i) * 2 * rows + 32, 32), 2 * rows), :] = gate.astype(F32)
         qt = (res[:, :128] * HEAD ** (-0.5)).T.astype(BF16)
 
         spot = pl.ds(pl.multiple_of((p % 2) * 2 * rows, 2 * rows), 2 * rows)
@@ -374,16 +385,6 @@
         @pl.when(p == NY - 1)
         def _():
             rcopy_rim.start()
-
-        for t, zt in ((1, (z + 1) % nz), (2, (z + nz - 1) % nz)):
-
-            @pl.when(among("k", t, zt))
-            def _(t=t, zt=zt):
-                kcopy(z, t, zt, here, i).start()
-
-            @pl.when(among("v", t, zt))
-            def _(t=t, zt=zt):
-                vcopy(z, t, zt, here, i).start()
 
         @pl.when(p // 2 == ha)
         def _():
@@ -835,28 +836,38 @@
     both_r.wait_recv()
     both_l.wait_recv()
     po[y] = po[y] + frl[...].astype(F32) + frr[...].astype(F32)
-    for t in range(8):
-        rcopy(
+    def from_tp(t):
+        return rcopy(
             at_out.at[0],
-            at_in.at[:, pl.ds(t * 2 * HEAD, 2 * HEAD)],
+            at_in.at[:, pl.ds(pl.multiple_of(t * 2 * HEAD, 2 * HEAD), 2 * HEAD)],
             asend.at[0],
             arecv.at[t],
             sp_of(zbar),
-        ).wait_recv()
-
-    lhs = at_in[...]
-
+        )
+
+    def last(part, emit):
+        for k in range(4):
+            from_tp(4 * part + k).wait_recv()
+        lhs = at_in[:, pl.ds(pl.multiple_of(part * 8 * HEAD, 8 * HEAD), 8 * HEAD)]
+
+        def columns(n, carry):
+            cols = pl.ds(pl.multiple_of(n * 512, 512), 512)
+            w = wo[pl.ds(4 * part, 4), :, cols].reshape(8 * HEAD, 512)
+            emit(cols, po[y, :, cols] + jnp.dot(lhs, w, preferred_element_type=F32))
+            return carry
+
+        lax.fori_loop(0, depth // 512, columns, 0)
+
+    def keep(cols, value):
+        po[y, :, cols] = value
+
+    def put(cols, value):
+        mixed[:, cols] = value.astype(BF16)
+
+    last(ha, keep)
+    last(hb, put)
     lcopy.wait_recv()
     log_total[:, pl.ds(pl.multiple_of(hb * mid_tok, mid_tok), mid_tok)] = lt_in[0:2, :]
-
-    def last(n, carry):
-        cols = pl.ds(pl.multiple_of(n * 512, 512), 512)
-        w = wo[:, :, cols].reshape(lhs.shape[1], 512)
-        res = jnp.dot(lhs, w, preferred_element_type=F32)
-        mixed[:, cols] = (po[y, :, cols] + res).astype(BF16)
-        return carry
-
-    lax.fori_loop(0, depth // 512, last, 0)
 
     for cp in g + gw:
         cp.wait_send()

time: 66.8 us -> 66 us (0.988)
  Pallas kernels: 64.8 us -> 64 us
    pallas_call x1, Pallas kernels: 64.8 us -> 64 us  [per_device(): pl.pallas_call(kernel, out_shape=(pltpu.VMEM((rows, depth), BF16), pltpu....]
where the time goes in v6:
time: 66 us; the launch traced here: 65.9 us
  Pallas kernels  64 us (97%)
  local copies, waits for them, and re-layouts  1.3 us (2%)
    pallas_call x1, Pallas kernels, per_device(): pl.pallas_call(kernel, out_shape=(pltpu.VMEM((rows, depth), BF16), pltpu....  64 us

profile of v6, /device:TPU:1, one launch (start us, length us, event | category | flops | bytes accessed | tf_op | source)
XLA Modules:
  0.0 65.9 jit_solution(10432649888285662457)
XLA Ops:
  0.6 64.0 %layer.1 = (bf16[64,2048]{1,0:T(8,128)(2,1)S(1)}, f32[2,512]{1,0:T(2,128)S(1)}) custom-call(bf16[64,2048]{1,0:T(8,128)(2,1)} %tokens.1, f32[1,2048]{1,0:T(1,128)} %bitcast.2, bf16[2048,128]{1,0:T(8,128)(2,1)} %w_query.1, bf16[2048,128]{1,0:T(8,128)(2,1)} %w_key.1, bf16[2048,128]{1,0:T(8,128)(2,1)} %w_value.1, bf16[2048,256]{1,0:T(8,128)(2,1)} %conv_in.1, ...), custom_call_target="tpu_custom_call" | custom-call | tf_op jit(solution)/shard_map/layer/pallas_call | solution.py:961
  64.6 0.7 %copy.16 = bf16[64,2048]{1,0:T(8,128)(2,1)} copy(bf16[64,2048]{1,0:T(8,128)(2,1)S(1)} %get-tuple-element.2) | data formatting | bytes 524288
  65.3 0.6 copy.17

commit v7 on v6

--- a/solution.py
+++ b/solution.py
@@ -934,8 +934,8 @@
         pltpu.VMEM((NX, 2, VROWS, tok), F32),
         pltpu.VMEM((NX - 1, att, tok), BF16),
         pltpu.VMEM((NX - 1, att, tok), BF16),
-        pltpu.VMEM((NX - 1, 8, tok), F32),
-        pltpu.VMEM((NX - 1, 8, tok), F32),
+        pltpu.VMEM((NX - 1, 4, tok), F32),
+        pltpu.VMEM((NX - 1, 4, tok), F32),
         pltpu.VMEM((tok, ch), BF16),
         pltpu.VMEM((32, ch), BF16),
         pltpu.VMEM((tok + 32, ch), F32),

time: 66 us -> 65.8 us (level)
  no operation moved by 1% of the time
where the time goes in v7:
time: 65.8 us; the launch traced here: 65.7 us
  Pallas kernels  63.8 us (97%)
  local copies, waits for them, and re-layouts  1.3 us (2%)
    pallas_call x1, Pallas kernels, per_device(): pl.pallas_call(kernel, out_shape=(pltpu.VMEM((rows, depth), BF16), pltpu....  63.8 us

profile of v7, /device:TPU:1, one launch (start us, length us, event | category | flops | bytes accessed | tf_op | source)
XLA Modules:
  0.0 65.7 jit_solution(11783408273190599672)
XLA Ops:
  0.6 63.8 %layer.1 = (bf16[64,2048]{1,0:T(8,128)(2,1)S(1)}, f32[2,512]{1,0:T(2,128)S(1)}) custom-call(bf16[64,2048]{1,0:T(8,128)(2,1)} %tokens.1, f32[1,2048]{1,0:T(1,128)} %bitcast.2, bf16[2048,128]{1,0:T(8,128)(2,1)} %w_query.1, bf16[2048,128]{1,0:T(8,128)(2,1)} %w_key.1, bf16[2048,128]{1,0:T(8,128)(2,1)} %w_value.1, bf16[2048,256]{1,0:T(8,128)(2,1)} %conv_in.1, ...), custom_call_target="tpu_custom_call" | custom-call | tf_op jit(solution)/shard_map/layer/pallas_call | solution.py:961
  64.4 0.7 %copy.16 = bf16[64,2048]{1,0:T(8,128)(2,1)} copy(bf16[64,2048]{1,0:T(8,128)(2,1)S(1)} %get-tuple-element.2) | data formatting | bytes 524288
  65.1 0.6 copy.17
